TPU v7x, 128 devices: a whole 4x4x4 slice. The times are simulated.
128 devices in a mesh: sp: 32 (over z, y, core), tp: 4 (over x).
Axes of the slice: x: 4, y: 4, z: 4, core: 2. Of those that a mesh axis runs over, the one named last changes fastest.
Arguments:
- queries: bfloat16 [16384, 512], P('sp', 'tp'), may hold values from -6 to 6
- key_matrix: bfloat16 [16384, 512], P('sp', 'tp'), may hold values from -6 to 6
- value_matrix: bfloat16 [16384, 1024], P('sp', 'tp'), may hold values from -6 to 6
- channel_decay_input: bfloat16 [16384, 512], P('sp', 'tp')
- head_decay_offset: float32 [16384, 8], P('sp', 'tp'), may hold values from -1 to 0
- output_gate_input: bfloat16 [16384, 1024], P('sp', 'tp'), may hold values from -6 to 6
- head_norm_gain: float32 [128], replicated, may hold values from 0.1 to 1.9
- residual: bfloat16 [16384, 2048], P(('sp', 'tp')), may hold values from -6 to 6
- mixer_output_weight: bfloat16 [1024, 2048], replicated, may hold values from -0.1875 to 0.1875
- expert_norm_gain: float32 [2048], replicated, may hold values from 0.1 to 1.9
- routes: int32 [16384, 4], P(('sp', 'tp')), may hold values from 0 to 255, all different within a row; in each aligned block of 128 rows (0 to 127, 128 to 255, ...) at most 4 rows name the same one
- chosen_router_scores: float32 [16384, 4], P(('sp', 'tp')), may hold values from 0.1 to 1
- routed_gate_weight: bfloat16 [256, 2048, 512], P(('sp', 'tp')), may hold values from -0.125 to 0.125
- routed_up_weight: bfloat16 [256, 2048, 512], P(('sp', 'tp')), may hold values from -0.125 to 0.125
- routed_down_weight: bfloat16 [256, 512, 2048], P(('sp', 'tp')), may hold values from -0.25 to 0.25
- common_gate_weight: bfloat16 [2048, 512], replicated, may hold values from -0.125 to 0.125
- common_up_weight: bfloat16 [2048, 512], replicated, may hold values from -0.125 to 0.125
- common_down_weight: bfloat16 [512, 2048], replicated, may hold values from -0.25 to 0.25
Outputs:
- layer_out: bfloat16 [16384, 2048], P(('sp', 'tp'))
Inputs may be any that keep to these rules, and one draw needn't show every extreme that they name: `routes`: each row names 4 different experts. In each aligned block of 128 rows (the rows of one device) no expert is named by more than 4 rows, a bound that some block reaches.
All inputs are finite; a program needn't handle non-finite values.
Results may differ from a plain program's by a relative error of at most 0.017.
Values may be sent and summed in bfloat16 or wider, within the bound.
A program may use at most 128 MiB of HBM per device.

v0:
```python
import jax
import jax.numpy as jnp
from jax import lax
from jax.sharding import Mesh
from jax.sharding import PartitionSpec as P

D = 2048
KEY_CHANNELS = 64
VDIM = 128
BLOCK = 64
TOP_K = 4
SP = ("sp_0", "sp_1", "sp_2")
SP_TP = ("sp_0", "sp_1", "sp_2", "tp")


eps_norm = 1e-06
decay_running = 16.0
routed_scale = 2.5


def filled_with(shard, identity):
    return jax.tree.map(
        lambda a, e: jnp.broadcast_to(jnp.asarray(e, a.dtype), a.shape), shard, identity
    )


def collected_together(shard, axis):
    leaves = jax.tree.leaves(shard)
    sequence = sorted(range(len(leaves)), key=lambda k: -leaves[k].size)
    width = (1, *leaves[sequence[0]].shape)[-1]
    lines = [
        jnp.pad(leaves[k].reshape(-1), (0, -leaves[k].size % width)).reshape(-1, width)
        for k in sequence
    ]
    both, at, found = (lax.all_gather(jnp.concatenate(lines), axis), 0, {})
    for k, line in zip(sequence, lines):
        section = both[:, at : at + len(line)].reshape(len(both), -1)
        found[k] = section[:, : leaves[k].size].reshape(-1, *leaves[k].shape)
        at += len(line)
    numbers = iter(range(len(leaves)))
    return jax.tree.map(lambda _: found[next(numbers)], shard)


def prefix_by_axis(shard, axes, combine, identity):
    before = start = filled_with(shard, identity)
    running = shard
    for axis in reversed(axes):
        size, mine = (lax.axis_size(axis), lax.axis_index(axis))
        pieces = collected_together(running, axis)
        inside, running = (start, start)
        for k in range(size):
            passed = k < mine
            running = combine(running, jax.tree.map(lambda part: part[k], pieces))
            inside = jax.tree.map(lambda new, old: jnp.where(passed, new, old), running, inside)
        before = combine(inside, before)
    return before


def expert_block(picked_rows, gate_weight, up_weight, down_weight):
    gate_pre = jnp.dot(picked_rows, gate_weight, preferred_element_type=jnp.float32)
    up_pre = jnp.dot(picked_rows, up_weight, preferred_element_type=jnp.float32)
    hidden = (jax.nn.silu(gate_pre) * up_pre).astype(jnp.bfloat16)
    return jnp.dot(hidden, down_weight, preferred_element_type=jnp.float32)


def apply_experts(arrived, routed_gate_weight, routed_up_weight, routed_down_weight):
    gate_pre = jnp.einsum(
        "sech,ehf->secf", arrived, routed_gate_weight, preferred_element_type=jnp.float32
    )
    up_pre = jnp.einsum(
        "sech,ehf->secf", arrived, routed_up_weight, preferred_element_type=jnp.float32
    )
    hidden = (jax.nn.silu(gate_pre) * up_pre).astype(jnp.bfloat16)
    return jnp.einsum(
        "secf,efh->sech", hidden, routed_down_weight, preferred_element_type=jnp.float32
    ).astype(jnp.bfloat16)


def chain_join(earlier, latter):
    return (earlier[0] * latter[0], latter[0][..., None] * earlier[1] + latter[1])


def on_device(
    queries,
    key_matrix,
    value_matrix,
    channel_decay_input,
    head_decay_offset,
    output_gate_input,
    head_norm_gain,
    residual,
    mixer_output_weight,
    expert_norm_gain,
    routes,
    chosen_router_scores,
    routed_gate_weight,
    routed_up_weight,
    routed_down_weight,
    common_gate_weight,
    common_up_weight,
    common_down_weight,
):
    device_heads = head_decay_offset.shape[1]
    seq_rows = queries.shape[0]
    blocks = seq_rows // BLOCK

    def split_local(values, columns):
        return (
            values.astype(jnp.float32)
            .reshape(blocks, BLOCK, device_heads, columns)
            .transpose(2, 0, 1, 3)
        )

    decay_spike_columns = jnp.repeat(head_decay_offset, KEY_CHANNELS, axis=1)
    decay_logarithm = (
        jax.nn.log_sigmoid(channel_decay_input.astype(jnp.float32)) / decay_running
        + decay_spike_columns
    )
    within = jnp.cumsum(split_local(decay_logarithm, KEY_CHANNELS), axis=2)
    block_end = within[:, :, -1, :]
    q_heads = split_local(queries, KEY_CHANNELS) * KEY_CHANNELS ** (-0.5)
    k_heads = split_local(key_matrix, KEY_CHANNELS)
    v_heads = split_local(value_matrix, VDIM)
    q_decay = q_heads * jnp.exp(within)
    k_grow = k_heads * jnp.exp(-within)
    k_tail = k_heads * jnp.exp(block_end[:, :, None, :] - within)
    causal = jnp.tril(jnp.ones((BLOCK, BLOCK), dtype=bool))
    scores = jnp.where(causal, jnp.einsum("hnid,hnjd->hnij", q_decay, k_grow), 0.0)
    inside = jnp.einsum("hnij,hnje->hnie", scores, v_heads)
    block_state = jnp.einsum("hncd,hnce->hnde", k_tail, v_heads)
    inclusive = jnp.cumsum(block_end, axis=1)
    exclusive = inclusive - block_end
    before = jnp.arange(blocks)[:, None] > jnp.arange(blocks)[None, :]
    spread = jnp.exp(
        jnp.where(
            before[None, :, :, None], exclusive[:, :, None, :] - inclusive[:, None, :, :], -jnp.inf
        )
    )
    local_start = jnp.einsum("hnmd,hmde->hnde", spread, block_state)
    total_log = inclusive[:, -1, :]
    tail_weight = jnp.exp(total_log[:, None, :] - inclusive)
    device_state = jnp.einsum("hnd,hnde->hde", tail_weight, block_state)
    device_decay = jnp.exp(total_log)
    identity = (jnp.ones_like(device_decay), jnp.zeros_like(device_state))
    _, carried = prefix_by_axis((device_decay, device_state), SP, chain_join, identity)
    entering = local_start + jnp.exp(exclusive)[..., None] * carried[:, None, :, :]
    output = inside + jnp.einsum("hncd,hnde->hnce", q_decay, entering)
    output = output.transpose(1, 2, 0, 3).reshape(seq_rows, device_heads, VDIM)
    inv_rms = lax.rsqrt(jnp.mean(output * output, axis=-1, keepdims=True) + eps_norm)
    normed_heads = (output * inv_rms * head_norm_gain).reshape(seq_rows, device_heads * VDIM)
    gated_output = (normed_heads * jax.nn.silu(output_gate_input.astype(jnp.float32))).astype(
        jnp.bfloat16
    )
    tok_count = residual.shape[0]
    stacked = gated_output.reshape(lax.axis_size("tp"), tok_count, gated_output.shape[1])
    projected = jnp.dot(
        lax.all_to_all(stacked, "tp", split_axis=0, concat_axis=2, tiled=True)[0],
        mixer_output_weight,
        preferred_element_type=jnp.float32,
    )[None][0]
    middle = (residual.astype(jnp.float32) + projected).astype(jnp.bfloat16)
    middle_wide = middle.astype(jnp.float32)
    norm_scale = lax.rsqrt(jnp.mean(middle_wide * middle_wide, axis=-1, keepdims=True) + eps_norm)
    normed = (middle_wide * norm_scale * expert_norm_gain).astype(jnp.bfloat16)
    weights = (
        routed_scale * chosen_router_scores / jnp.sum(chosen_router_scores, axis=-1, keepdims=True)
    )
    devices = lax.axis_size(SP) * lax.axis_size("tp")
    exp_dev = routed_gate_weight.shape[0]
    experts_all = exp_dev * devices
    cap_slots = 2 * TOP_K * tok_count // experts_all
    flat_expert = routes.reshape(-1)
    one_hot = (flat_expert[:, None] == jnp.arange(experts_all, dtype=jnp.int32)[None, :]).astype(
        jnp.int32
    )
    slot_index = jnp.sum((jnp.cumsum(one_hot, axis=0) - 1) * one_hot, axis=1)
    destination = flat_expert * cap_slots + slot_index
    buffer_rows = experts_all * cap_slots
    row_owner = jnp.arange(flat_expert.shape[0], dtype=jnp.int32) // TOP_K
    source_row = jnp.full((buffer_rows,), tok_count, jnp.int32).at[destination].set(row_owner)
    normed_pad = jnp.concatenate([normed, jnp.zeros((1, D), jnp.bfloat16)], axis=0)
    outgoing = normed_pad[source_row].reshape(devices, exp_dev, cap_slots, D)
    produced = apply_experts(
        lax.all_to_all(outgoing, SP_TP, split_axis=0, concat_axis=0, tiled=True),
        routed_gate_weight,
        routed_up_weight,
        routed_down_weight,
    )
    returned = lax.all_to_all(produced, SP_TP, split_axis=0, concat_axis=0, tiled=True)
    flat_back = returned.reshape(buffer_rows, D)
    gathered = flat_back[destination].reshape(tok_count, TOP_K, D)
    routed = jnp.sum(weights[:, :, None] * gathered, axis=1)
    shared = expert_block(normed, common_gate_weight, common_up_weight, common_down_weight)
    return (middle_wide + routed + shared).astype(jnp.bfloat16)


def solution(mesh):
    torus = Mesh(mesh.devices.reshape(4, 4, 2, mesh.shape["tp"]), ("sp_0", "sp_1", "sp_2", "tp"))
    return jax.shard_map(
        on_device,
        mesh=torus,
        in_specs=(
            P(SP, "tp"),
            P(SP, "tp"),
            P(SP, "tp"),
            P(SP, "tp"),
            P(SP, "tp"),
            P(SP, "tp"),
            P(),
            P(SP_TP, None),
            P(),
            P(),
            P(SP_TP, None),
            P(SP_TP, None),
            P(SP_TP, None, None),
            P(SP_TP, None, None),
            P(SP_TP, None, None),
            P(),
            P(),
            P(),
        ),
        out_specs=P(SP_TP, None),
        check_vma=False,
    )
```

profile of v0, /device:TPU:1, one launch (start us, length us, event | category | flops | bytes accessed | tf_op | source)
XLA Modules:
  0.0 278.0 jit_solution(1832661175801430715)
XLA Ops:
  8.5 2.0 bitcast_multiply_fusion.3
  12.0 2.9 %all-gather.3 = f32[2,129,128]{2,1,0:T(8,128)S(1)} all-gather(f32[1,129,128]{2,1,0:T(8,128)S(1)} %maximum_bitcast_fusion), channel_id=2, replica_groups=mesh['sp_0'=4,'sp_1'=4,'sp_2'=2,'tp'=4] {'sp_2'}, dimensions={0}, use_global_device_ids=true | all-gather | bytes 198144 | tf_op jit(solution)/shard_map/all_gather | solution.py:35
  15.6 10.5 %all-gather.4 = f32[4,129,128]{2,1,0:T(8,128)S(1)} all-gather(f32[1,129,128]{2,1,0:T(8,128)S(1)} %maximum_bitcast_fusion.1), channel_id=3, replica_groups=mesh['sp_0'=4,'sp_1'=4,'sp_2'=2,'tp'=4] {'sp_1'}, dimensions={0}, use_global_device_ids=true | all-gather | bytes 330240 | tf_op jit(solution)/shard_map/all_gather | solution.py:35
  26.9 10.6 %all-gather.5 = f32[4,129,128]{2,1,0:T(8,128)S(1)} all-gather(f32[1,129,128]{2,1,0:T(8,128)S(1)} %maximum_bitcast_fusion.2), channel_id=4, replica_groups=mesh['sp_0'=4,'sp_1'=4,'sp_2'=2,'tp'=4] {'sp_0'}, dimensions={0}, use_global_device_ids=true | all-gather | bytes 330240 | tf_op jit(solution)/shard_map/all_gather | solution.py:35
  41.4 1.3 squeeze.68
  45.2 1.3 squeeze.67
  46.5 1.3 squeeze.72
  47.8 1.3 squeeze.71
  50.4 1.3 mul.445
  54.2 1.4 copy.54
  57.4 1.4 add_add_fusion.1
  58.8 1.4 fusion.27
  61.4 1.5 copy.60
  66.1 4.0 %all-to-all-start = ((bf16[4,128,256]{1,2,0:T(8,128)(2,1)}), bf16[4,128,256]{1,2,0:T(8,128)(2,1)S(1)}, u32[]{:S(2)}, u32[]{:S(2)}) async-start(bf16[4,128,256]{1,2,0:T(8,128)(2,1)} %copy.62), calls=%async_computation | async-start | bytes 524288 | tf_op jit(solution)/shard_map/all_to_all | solution.py:157
  71.5 2.4 scatter_custom_fusion
  74.0 1.6 all-to-all-done
  75.6 3.0 %multiply_reduce_fusion.1 = (f32[128]{0:T(128)S(1)}, f32[128,2048]{1,0:T(8,128)S(1)}) fusion(bf16[128,1024]{0,1:T(8,128)(2,1)S(1)} %bitcast.188, bf16[1024,2048]{1,0:T(8,128)(2,1)} %param.26, bf16[128,2048]{1,0:T(8,128)(2,1)S(1)} %copy-done.5), kind=kOutput, calls=%fused_computation.35 | convolution fusion | flops 538443648 | bytes 6029824 | tf_op jit(solution)/shard_map/dot_general | solution.py:156
  79.9 6.0 %gather_fusion = bf16[1024,2048]{1,0:T(8,128)(2,1)} fusion(bf16[129,2048]{1,0:T(8,128)(2,1)S(1)} %concatenate.15, s32[1024]{0:T(1024)S(1)} %fusion.80), kind=kCustom, calls=%fused_computation | custom fusion | bytes 8392704 | tf_op jit(solution)/shard_map/gather | solution.py:182
  85.9 7.2 %reshape.433 = bf16[128,2,4,2048]{3,2,1,0:T(4,128)(2,1)} reshape(bf16[1024,2048]{1,0:T(8,128)(2,1)} %gather_fusion) | data formatting | bytes 8388608 | tf_op jit(solution)/shard_map/reshape | solution.py:182
  93.1 66.9 %all_to_all.25 = bf16[128,2,4,2048]{3,2,1,0:T(4,128)(2,1)S(1)} all-to-all(bf16[128,2,4,2048]{3,2,1,0:T(4,128)(2,1)} %reshape.433), channel_id=1, replica_groups=mesh['sp_0'=4,'sp_1'=4,'sp_2'=2,'tp'=4] {'sp_0','sp_1','sp_2','tp'}, dimensions={0} | all-to-all | bytes 8388608 | tf_op jit(solution)/shard_map/all_to_all | solution.py:184
  160.0 2.0 copy-done.4
  161.9 6.1 %fusion.4 = f32[2,128,4,512]{3,1,2,0:T(8,128)} fusion(bf16[2,2048,512]{2,1,0:T(8,128)(2,1)S(1)} %copy-done.12, bf16[128,2,4,2048]{3,2,1,0:T(4,128)(2,1)S(1)} %all_to_all.25), kind=kOutput, calls=%fused_computation.7 | convolution fusion | flops 2147483648 | bytes 10485760 | tf_op jit(solution)/shard_map/sech,ehf->secf/dot_general | solution.py:67
  168.1 14.4 %convert_bitcast_fusion = bf16[128,2,4,2048]{3,0,2,1:T(8,128)(2,1)} fusion(bf16[2,512,2048]{2,1,0:T(8,128)(2,1)} %param.32, f32[2,128,4,512]{3,1,2,0:T(8,128)} %fusion.4, bf16[2,2048,512]{2,1,0:T(8,128)(2,1)} %param.31, bf16[128,2,4,2048]{3,2,1,0:T(4,128)(2,1)} %copy-done.4), kind=kOutput, calls=%fused_computation.10 | convolution fusion | flops 4300210176 | bytes 18874368 | tf_op jit(solution)/shard_map/secf,efh->sech/dot_general | solution.py:74
  182.4 7.6 %copy.71 = bf16[128,2,4,2048]{3,2,1,0:T(4,128)(2,1)} copy(bf16[128,2,4,2048]{3,0,2,1:T(8,128)(2,1)} %convert_bitcast_fusion) | data formatting | bytes 8388608 | tf_op jit(solution)/shard_map/convert_element_type | solution.py:76
  190.1 5.2 %all-to-all-start.2 = ((bf16[128,2,4,2048]{3,2,1,0:T(4,128)(2,1)}), bf16[128,2,4,2048]{3,2,1,0:T(4,128)(2,1)}, u32[]{:S(2)}, u32[]{:S(2)}) async-start(bf16[128,2,4,2048]{3,2,1,0:T(4,128)(2,1)} %copy.71), calls=%async_computation.2 | async-start | bytes 8388608 | tf_op jit(solution)/shard_map/all_to_all | solution.py:189
  195.4 2.0 fusion.95
  197.4 50.9 %all-to-all-done.2 = bf16[128,2,4,2048]{3,2,1,0:T(4,128)(2,1)} async-done(((bf16[128,2,4,2048]{3,2,1,0:T(4,128)(2,1)}), bf16[128,2,4,2048]{3,2,1,0:T(4,128)(2,1)}, u32[]{:S(2)}, u32[]{:S(2)}) %all-to-all-start.2) | async-done | bytes 4194336 | tf_op jit(solution)/shard_map/all_to_all | solution.py:189
  248.4 6.9 %reshape.434 = bf16[1024,2048]{1,0:T(8,128)(2,1)} reshape(bf16[128,2,4,2048]{3,2,1,0:T(4,128)(2,1)} %all-to-all-done.2) | data formatting | bytes 8388608 | tf_op jit(solution)/shard_map/reshape | solution.py:190
  255.3 8.0 %gather_fusion.1 = bf16[512,2048]{1,0:T(8,128)(2,1)} fusion(bf16[1024,2048]{1,0:T(8,128)(2,1)} %reshape.434, s32[1024]{0:T(1024)S(1)} %pad_clamp_fusion), kind=kCustom, calls=%fused_computation.1 | custom fusion | bytes 4196352 | tf_op jit(solution)/shard_map/gather | solution.py:191
  263.2 4.8 %reshape.435 = f32[128,4,2048]{2,1,0:T(4,128)} reshape(bf16[512,2048]{1,0:T(8,128)(2,1)} %gather_fusion.1) | data formatting | bytes 6291456 | tf_op jit(solution)/shard_map/convert_element_type | solution.py:192
  268.0 6.4 %multiply_reduce_fusion = f32[128,2048]{1,0:T(8,128)} fusion(f32[128,4,2048]{2,1,0:T(4,128)} %reshape.435, f32[128,4]{1,0:T(8,128)S(1)} %copy.63), kind=kLoop, calls=%fused_computation.9 | loop fusion | flops 1835008 | bytes 5244928 | tf_op jit(solution)/shard_map/reduce_sum | solution.py:192
  274.4 3.7 %fusion.12 = bf16[128,2048]{1,0:T(8,128)(2,1)} fusion(bf16[512,2048]{1,0:T(8,128)(2,1)S(1)} %copy-done, bf16[128,2048]{1,0:T(8,128)(2,1)} %copy-done.3, bf16[2048,512]{1,0:T(8,128)(2,1)} %param.34, f32[128,2048]{1,0:T(8,128)S(1)} %copy-done.2, f32[128,2048]{1,0:T(8,128)} %multiply_reduce_fusion, f32[128,512]{1,0:T(8,128)S(1)} %fusion.95), kind=kOutput, calls=%fused_computation.17 | convolution fusion | flops 538050560 | bytes 7602176 | tf_op jit(solution)/shard_map/dot_general | solution.py:63
  (97 shorter events, 30.4 us)
Async XLA Ops:
  0.0 274.4 %copy-start = (bf16[512,2048]{1,0:T(8,128)(2,1)S(1)}, bf16[512,2048]{1,0:T(8,128)(2,1)}, u32[]{:S(2)}) copy-start(bf16[512,2048]{1,0:T(8,128)(2,1)} %param.35) | copy-start | bytes 6291460
  0.0 7.2 %copy-start.8 = (bf16[512,128]{1,0:T(8,128)(2,1)S(1)}, bf16[512,128]{1,0:T(8,128)(2,1)}, u32[]{:S(2)}) copy-start(bf16[512,128]{1,0:T(8,128)(2,1)} %param.19) | copy-start | bytes 393220
  0.0 8.3 %copy-start.7 = (bf16[512,256]{1,0:T(8,128)(2,1)S(1)}, bf16[512,256]{1,0:T(8,128)(2,1)}, u32[]{:S(2)}) copy-start(bf16[512,256]{1,0:T(8,128)(2,1)} %param.20) | copy-start | bytes 786436
  10.7 28.8 %copy-start.6 = (bf16[2,8,64,128]{3,2,1,0:T(8,128)(2,1)}, bf16[2,8,64,128]{3,2,1,0:T(8,128)(2,1)S(1)}, u32[]{:S(2)}) copy-start(bf16[2,8,64,128]{3,2,1,0:T(8,128)(2,1)S(1)} %fusion.39) | copy-start | bytes 786436
  58.8 11.3 %copy-start.10 = (s32[128,4]{0,1:T(4,128)S(1)}, s32[128,4]{0,1:T(4,128)}, u32[]{:S(2)}) copy-start(s32[128,4]{0,1:T(4,128)} %param.28) | copy-start | bytes 6148
  61.3 14.4 %copy-start.5 = (bf16[128,2048]{1,0:T(8,128)(2,1)S(1)}, bf16[128,2048]{1,0:T(8,128)(2,1)}, u32[]{:S(2)}) copy-start(bf16[128,2048]{1,0:T(8,128)(2,1)} %param.25) | copy-start | bytes 1572868
  66.1 9.5 %all-to-all-start = ((bf16[4,128,256]{1,2,0:T(8,128)(2,1)}), bf16[4,128,256]{1,2,0:T(8,128)(2,1)S(1)}, u32[]{:S(2)}, u32[]{:S(2)}) async-start(bf16[4,128,256]{1,2,0:T(8,128)(2,1)} %copy.62), calls=%async_computation | async-start | bytes 524288 | tf_op jit(solution)/shard_map/all_to_all | solution.py:157
  70.8 8.8 %copy-start.9 = (f32[2048]{0:T(1024)S(1)}, f32[2048]{0:T(1024)}, u32[]{:S(2)}) copy-start(f32[2048]{0:T(1024)} %param.27) | copy-start | bytes 24580
  78.7 1.0 copy-start.1
  79.8 115.6 %copy-start.3 = (bf16[128,2048]{1,0:T(8,128)(2,1)}, bf16[128,2048]{1,0:T(8,128)(2,1)S(1)}, u32[]{:S(2)}) copy-start(bf16[128,2048]{1,0:T(8,128)(2,1)S(1)} %multiply_convert_fusion) | copy-start | bytes 1572868
  93.1 68.8 %copy-start.12 = (bf16[2,2048,512]{2,1,0:T(8,128)(2,1)S(1)}, bf16[2,2048,512]{2,1,0:T(8,128)(2,1)}, u32[]{:S(2)}) copy-start(bf16[2,2048,512]{2,1,0:T(8,128)(2,1)} %param.30) | copy-start | bytes 12582916
  160.0 2.0 copy-start.4
  190.0 5.2 %copy-start.11 = (f32[128,4]{0,1:T(4,128)S(1)}, f32[128,4]{0,1:T(4,128)}, u32[]{:S(2)}) copy-start(f32[128,4]{0,1:T(4,128)} %param.29) | copy-start | bytes 6148
  190.1 58.3 %all-to-all-start.2 = ((bf16[128,2,4,2048]{3,2,1,0:T(4,128)(2,1)}), bf16[128,2,4,2048]{3,2,1,0:T(4,128)(2,1)}, u32[]{:S(2)}, u32[]{:S(2)}) async-start(bf16[128,2,4,2048]{3,2,1,0:T(4,128)(2,1)} %copy.71), calls=%async_computation.2 | async-start | bytes 8388608 | tf_op jit(solution)/shard_map/all_to_all | solution.py:189
  268.0 6.4 %copy-start.2 = (f32[128,2048]{1,0:T(8,128)S(1)}, f32[128,2048]{1,0:T(8,128)}, u32[]{:S(2)}) copy-start(f32[128,2048]{1,0:T(8,128)} %copy-done.1) | copy-start | bytes 3145732
where the time goes:
time: 279 us; the launch traced here: 278 us
  blocking collectives  90.9 us (33%)
  local copies, waits for them, and re-layouts  73 us (26%)
  waiting for transfers between devices  52.6 us (19%)
  matrix products  33.5 us (12%)
  other arithmetic  18.5 us (7%)
  starting transfers between devices  9.16 us (3%)
    all_to_all x1, blocking collectives, on_device(): lax.all_to_all(outgoing, SP_TP, split_axis=0, concat_axis=0, tiled=True)  66.9 us
    all_to_all x1, waiting for transfers between devices, on_device(): lax.all_to_all(produced, SP_TP, split_axis=0, concat_axis=0, tiled=True)  50.9 us
    all_gather x3, blocking collectives, collected_together(): both, at, found = (lax.all_gather(jnp.concatenate(lines), axis), 0, {})  24.1 us
    dot_general x1, matrix products, apply_experts(): jnp.einsum('secf,efh->sech', hidden, routed_down_weight, preferred_elemen...  14.4 us
    gather x1, local copies, waits for them, and re-layouts, on_device(): gathered = flat_back[destination].reshape(tok_count, TOP_K, D)  7.96 us
    squeeze x6, local copies, waits for them, and re-layouts, prefix_by_axis(): running = combine(running, jax.tree.map(lambda part: part[k], pieces))  7.69 us
    convert_element_type x1, local copies, waits for them, and re-layouts, apply_experts(): return jnp.einsum('secf,efh->sech', hidden, routed_down_weight, preferred...  7.61 us
    reshape x1, local copies, waits for them, and re-layouts, on_device(): outgoing = normed_pad[source_row].reshape(devices, exp_dev, cap_slots, D)  7.19 us
  transfers between devices with their start and end apart: 2, of which 2 were waited for; matrix products, arithmetic and copies ran while one was open for 2% of the time, Pallas kernels for 0%

commit v1 on v0

v1 whole, which is shorter than its diff:
```python
import jax
import jax.numpy as jnp
from jax import lax
from jax.experimental import pallas as pl
from jax.experimental.pallas import tpu as pltpu
from jax.sharding import PartitionSpec as P

MESH = pl.DeviceIdType.MESH
BF = jnp.bfloat16
F32 = jnp.float32
I32 = jnp.int32

BLOCK = 64
NZ, NY, NC, NX = 4, 4, 2, 4
DEVS = NZ * NY * NC * NX
STRIDE = 37
CHUNK = 32
CHUNKS = DEVS // CHUNK

EPS = 1e-6
RUNNING = 16.0
SCALE = 2.5


def dot(a, b):
    return jnp.dot(a, b, preferred_element_type=F32)


def dot_nt(a, b):
    return lax.dot_general(a, b, (((1,), (1,)), ((), ())), preferred_element_type=F32)


def dot_tn(a, b):
    return lax.dot_general(a, b, (((0,), (0,)), ((), ())), preferred_element_type=F32)


def silu(v):
    return v / (1.0 + jnp.exp(-v))


def three(v):
    hi = v.astype(BF)
    rest = v - hi.astype(F32)
    mid = rest.astype(BF)
    low = (rest - mid.astype(F32)).astype(BF)
    return hi, mid, low


def kernel(
    q_hbm, k_hbm, v_hbm, cd_hbm, hd_ref, og_hbm, hgain_ref, res_hbm, wo_hbm, egain_ref,
    routes_ref, scores_ref, wg_hbm, wu_hbm, wd_hbm, cg_hbm, cu_hbm, cdn_hbm,
    out_ref,
    q_s, k_s, v_s, cd_s, og_s, res_s, wo_s, wg_s, wu_s, wd_s, cg_s, cu_s, cdn_s,
    st1, st1r, st2, st3, outacc, qx_s, gsend, grecv, mid_s, nrm_s, shared_s,
    lhs_s, cw_s, send, recv, ret, back, acc_s,
    load_sem, s1, r1, s2, r2, s3, r3, gs, gr, ds, dr, es, er,
):
    sp = lax.axis_index("sp")
    x = lax.axis_index("tp")
    z = sp // (NY * NC)
    y = (sp // NC) % NY
    c = sp % NC

    def place(zz, yy, cc, xx):
        return ((zz % NZ) * (NY * NC) + (yy % NY) * NC + cc % NC, xx % NX)

    loads = [
        pltpu.make_async_copy(a, b, load_sem.at[n])
        for n, (a, b) in enumerate(
            (
                (cd_hbm, cd_s), (k_hbm, k_s), (v_hbm, v_s), (q_hbm, q_s), (og_hbm, og_s),
                (wo_hbm, wo_s), (res_hbm, res_s), (cg_hbm, cg_s), (cu_hbm, cu_s),
                (cdn_hbm, cdn_s), (wg_hbm, wg_s), (wu_hbm, wu_s), (wd_hbm, wd_s),
            )
        )
    ]
    for one in loads:
        one.start()
    (l_cd, l_k, l_v, l_q, l_og, l_wo, l_res, l_cg, l_cu, l_cdn, l_wg, l_wu, l_wd) = loads

    bar = pltpu.get_barrier_semaphore()
    neighbours = [place(z, y, c + 1, x)]
    neighbours += [place(z, y + d, c, x) for d in (1, 2, 3)]
    neighbours += [place(z + d, y, c, x) for d in (1, 2, 3)]
    neighbours += [place(z, y, c, x + d) for d in (1, 2, 3)]
    for one in neighbours:
        pl.semaphore_signal(bar, inc=1, device_id=one, device_id_type=MESH)

    lane = lax.broadcasted_iota(I32, (1, 128), 1)
    first = lane < 64
    rows_i = lax.broadcasted_iota(I32, (256, 256), 0)
    cols_i = lax.broadcasted_iota(I32, (256, 256), 1)
    causal = (rows_i >= cols_i) & ((rows_i >> 6) == (cols_i >> 6))
    tri = causal.astype(F32).astype(BF)
    hd = jnp.where(first, hd_ref[:, 0:1], hd_ref[:, 1:2])
    l_cd.wait()
    cd = cd_s[...].astype(F32)
    dl = (jnp.minimum(cd, 0.0) - jnp.log1p(jnp.exp(-jnp.abs(cd)))) / RUNNING + hd
    parts = three(dl)
    within = jnp.concatenate(
        [sum(dot(tri, p[256 * n : 256 * n + 256]) for p in parts) for n in (0, 1)], axis=0
    )
    w3 = within.reshape(8, BLOCK, 128)
    ends = [w3[n, BLOCK - 1 : BLOCK, :] for n in range(8)]
    incl = []
    running = jnp.zeros((1, 128), F32)
    for n in range(8):
        running = running + ends[n]
        incl.append(running)
    total = incl[7]
    excl3 = jnp.stack([incl[n] - ends[n] for n in range(8)], axis=0)
    ends3 = jnp.stack(ends, axis=0)

    l_k.wait()
    l_v.wait()
    k = k_s[...].astype(F32)
    k3 = k.reshape(8, BLOCK, 128)
    k_tt = (k3 * jnp.exp(total[None] - excl3 - w3)).reshape(512, 128).astype(BF)
    v0, v1 = v_s[:, 0:128], v_s[:, 128:256]
    own_state = jnp.where(first, dot_tn(v0, k_tt), dot_tn(v1, k_tt))

    row16 = lax.broadcasted_iota(I32, (16, 128), 0)

    def put_state(ref, log, state):
        ref[0:128, :] = state.astype(BF)
        hi, mid, low = (p.astype(F32) for p in three(log))
        tail = jnp.where(row16 == 0, hi, jnp.where(row16 == 1, mid, jnp.where(row16 == 2, low, 0.0)))
        ref[128:144, :] = tail.astype(BF)

    def get_state(ref):
        log = jnp.sum(ref[128:144, :].astype(F32), axis=0, keepdims=True)
        return log, ref[0:128, :].astype(F32)

    put_state(st1, total, own_state)
    pl.semaphore_wait(bar, 10)
    core_copy = pltpu.make_async_remote_copy(
        src_ref=st1, dst_ref=st1r, send_sem=s1, recv_sem=r1,
        device_id=place(z, y, c + 1, x), device_id_type=MESH,
    )
    core_copy.start()

    l_q.wait()
    ew = jnp.exp(within)
    qd = q_s[...].astype(F32) * 0.125 * ew
    qx_s[...] = (qd.reshape(8, BLOCK, 128) * jnp.exp(excl3)).reshape(512, 128).astype(BF)
    kg = (k * jnp.exp(-within)).astype(BF)
    for h in (0, 1):
        q_h = jnp.where(first if h == 0 else ~first, qd, 0.0).astype(BF)
        v_h = v0 if h == 0 else v1
        for n in (0, 1):
            sl = slice(256 * n, 256 * n + 256)
            scores = jnp.where(causal, dot_nt(q_h[sl], kg[sl]), 0.0).astype(BF)
            outacc[h, sl, :] = dot(scores, v_h[sl])

    core_copy.wait()
    core1 = c == 1
    log_p, state_p = get_state(st1r)
    pair_log = total + log_p
    pair_state = jnp.where(
        core1,
        jnp.exp(total) * state_p + own_state,
        jnp.exp(log_p) * own_state + state_p,
    )
    carry_log = jnp.where(core1, log_p, 0.0)
    carry_state = jnp.where(core1, state_p, 0.0)

    def exchange(slots, mine, log, state, ssem, rsem, target):
        put_state(slots.at[mine], log, state)
        copies = []
        for d in (1, 2, 3):
            one = pltpu.make_async_remote_copy(
                src_ref=slots.at[mine], dst_ref=slots.at[mine],
                send_sem=ssem.at[d], recv_sem=rsem.at[d],
                device_id=target(d), device_id_type=MESH,
            )
            one.start()
            copies.append(one)
        return copies

    def prefix(slots, mine, count, carry_log, carry_state):
        run_log = jnp.zeros((1, 128), F32)
        run_state = jnp.zeros((128, 128), F32)
        pre_log, pre_state = run_log, run_state
        for n in range(count):
            pre_log = jnp.where(mine == n, run_log, pre_log)
            pre_state = jnp.where(mine == n, run_state, pre_state)
            log, state = get_state(slots.at[n])
            run_state = jnp.exp(log) * run_state + state
            run_log = run_log + log
        carry_state = jnp.exp(carry_log) * pre_state + carry_state
        carry_log = carry_log + pre_log
        return run_log, run_state, carry_log, carry_state

    y_copies = exchange(st2, y, pair_log, pair_state, s2, r2, lambda d: place(z, y + d, c, x))

    k_tail = (k3 * jnp.exp(ends3 - w3)).reshape(512, 128).astype(BF)
    state = jnp.zeros((128, 128), F32)
    for n in range(8):
        sl = slice(BLOCK * n, BLOCK * n + BLOCK)
        if n > 0:
            state_b = state.astype(BF)
            for h in (0, 1):
                q_h = jnp.where(first if h == 0 else ~first, qd[sl], 0.0).astype(BF)
                outacc[h, sl, :] += dot_nt(q_h, state_b)
        if n < 7:
            added = jnp.where(first, dot_tn(v0[sl], k_tail[sl]), dot_tn(v1[sl], k_tail[sl]))
            state = jnp.exp(ends[n]) * state + added

    for one in y_copies:
        one.wait()
    plane_log, plane_state, carry_log, carry_state = prefix(st2, y, NY, carry_log, carry_state)
    z_copies = exchange(st3, z, plane_log, plane_state, s3, r3, lambda d: place(z + d, y, c, x))

    def expert_of(index):
        off = ((index >> 4) * STRIDE) & (DEVS - 1)
        dev = ((z + (off >> 5)) & 3) * 8 + ((y + (off >> 3)) & 3) * 2 + ((c + off) & 1)
        return (dev * 4 + ((x + (off >> 1)) & 3)) * 2 + ((index >> 2) & 1)

    routes = routes_ref[...].astype(F32)
    sub128 = lax.broadcasted_iota(I32, (128, 128), 0)
    lan128 = lax.broadcasted_iota(I32, (128, 128), 1)
    upper = (sub128 < lan128).astype(F32).astype(BF)
    lower = (sub128 > lan128).astype(F32).astype(BF)
    wide = jnp.zeros((128, 128), F32)
    for n in range(4):
        wide = jnp.where(lan128 == n, routes[:, n : n + 1], wide)
    turned = wide.T
    for n in range(8):
        q_index = lax.broadcasted_iota(I32, (256, 128), 0) + 256 * n
        expert = expert_of(q_index).astype(F32)
        match = jnp.zeros((256, 128), F32)
        for j in range(4):
            match = jnp.where(expert == turned[j : j + 1, :], 1.0, match)
        rank = dot(match.astype(BF), upper)
        live = jnp.where(rank == (q_index & 3).astype(F32), match, 0.0)
        half = ((q_index >> 3) & 1) == 0
        lhs_s[256 * n : 256 * n + 256, 0:128] = jnp.where(half, live, 0.0).astype(BF)
        lhs_s[256 * n : 256 * n + 256, 128:256] = jnp.where(half, 0.0, live).astype(BF)
    scores = scores_ref[...]
    weights = SCALE * scores / jnp.sum(scores, axis=-1, keepdims=True)
    for n in range(4):
        q_index = lax.broadcasted_iota(I32, (128, 512), 1) + 512 * n
        expert = expert_of(q_index).astype(F32)
        weight = jnp.zeros((128, 512), F32)
        match = jnp.zeros((128, 512), F32)
        for j in range(4):
            hit = expert == routes[:, j : j + 1]
            match = jnp.where(hit, 1.0, match)
            weight = jnp.where(hit, weights[:, j : j + 1], weight)
        rank = dot(lower, match.astype(BF))
        weight = jnp.where(rank == (q_index & 3).astype(F32), weight, 0.0)
        half = ((q_index >> 3) & 1) == 0
        cw_s[0:128, 512 * n : 512 * n + 512] = jnp.where(half, weight, 0.0).astype(BF)
        cw_s[128:256, 512 * n : 512 * n + 512] = jnp.where(half, 0.0, weight).astype(BF)

    for one in z_copies:
        one.wait()
    _, _, _, carried = prefix(st3, z, NZ, carry_log, carry_state)
    carried_b = carried.astype(BF)

    l_og.wait()
    g_copies = []
    for d in (1, 2, 3, 0):
        xx = (x + d) % NX
        rows = pl.ds(pl.multiple_of(xx * 128, 128), 128)
        qx = qx_s[rows, :]
        for h in (0, 1):
            q_h = jnp.where(first if h == 0 else ~first, qx.astype(F32), 0.0).astype(BF)
            attn = outacc[h, rows, :] + dot_nt(q_h, carried_b)
            inv = lax.rsqrt(jnp.mean(attn * attn, axis=-1, keepdims=True) + EPS)
            gate = og_s[rows, 128 * h : 128 * h + 128].astype(F32)
            value = attn * inv * hgain_ref[...] * silu(gate)
            gsend[d, :, 128 * h : 128 * h + 128] = value.astype(BF)
        if d > 0:
            one = pltpu.make_async_remote_copy(
                src_ref=gsend.at[d], dst_ref=grecv.at[d], send_sem=gs.at[d], recv_sem=gr.at[d],
                device_id=place(z, y, c, x + d), device_id_type=MESH,
            )
            one.start()
            g_copies.append(one)

    l_wo.wait()
    l_res.wait()
    w_rows = pl.ds(pl.multiple_of(x * 256, 256), 256)
    proj = dot(gsend[0], wo_s[w_rows, :])
    for d in (1, 2, 3):
        g_copies[d - 1].wait()
        w_rows = pl.ds(pl.multiple_of(((x + NX - d) % NX) * 256, 256), 256)
        proj = proj + dot(grecv[d], wo_s[w_rows, :])
    middle = (res_s[...].astype(F32) + proj).astype(BF)
    mid_s[...] = middle
    mid_w = middle.astype(F32)
    scale = lax.rsqrt(jnp.mean(mid_w * mid_w, axis=-1, keepdims=True) + EPS)
    normed = (mid_w * scale * egain_ref[...]).astype(BF)
    nrm_s[0:128, :] = normed[:, 0:1024]
    nrm_s[128:256, :] = normed[:, 1024:2048]

    def target(i, sign):
        k = (i * STRIDE) % DEVS
        return place(
            z + NZ + sign * (k // 32), y + NY + sign * ((k // 8) % 4),
            c + NC + sign * (k % 2), x + NX + sign * ((k // 2) % 4),
        )

    def send_copy(i):
        return pltpu.make_async_remote_copy(
            src_ref=send.at[i], dst_ref=recv.at[i],
            send_sem=ds.at[i // CHUNK], recv_sem=dr.at[i // CHUNK],
            device_id=target(i, 1), device_id_type=MESH,
        )

    def ret_copy(i):
        return pltpu.make_async_remote_copy(
            src_ref=ret.at[i], dst_ref=back.at[i],
            send_sem=es.at[i // CHUNK], recv_sem=er.at[i // CHUNK],
            device_id=target(i, -1), device_id_type=MESH,
        )

    def chunk_refs(first_slot, count, n, a, b, asem, bsem):
        return pltpu.make_async_remote_copy(
            src_ref=a.at[pl.ds(first_slot, count)], dst_ref=b.at[pl.ds(first_slot, count)],
            send_sem=asem.at[n], recv_sem=bsem.at[n],
            device_id=target(1, 1), device_id_type=MESH,
        )

    def start_range(make, lo, hi):
        def body(i, carry):
            make(i).start()
            return carry

        lax.fori_loop(lo, hi, body, 0)

    for n in range(8):
        rows = dot(lhs_s[256 * n : 256 * n + 256, :], nrm_s[...]).astype(BF).reshape(16, 16, 1024)
        send[16 * n : 16 * n + 16] = rows
        if n == 0:
            recv[0] = rows[0]
        start_range(send_copy, max(16 * n, 1), 16 * n + 16)

    l_cg.wait()
    l_cu.wait()
    l_cdn.wait()
    nrm = jnp.concatenate([nrm_s[0:128, :], nrm_s[128:256, :]], axis=1)
    hidden = (silu(dot(nrm, cg_s[...])) * dot(nrm, cu_s[...])).astype(BF)
    shared_s[...] = dot(hidden, cdn_s[...])

    l_wg.wait()
    l_wu.wait()
    l_wd.wait()
    pr = lax.broadcasted_iota(I32, (512, 512), 0)
    pc = lax.broadcasted_iota(I32, (512, 512), 1)
    want = ((pr >> 2) & 31) * 16 + ((pr >> 7) & 1) * 8 + (pr >> 8) * 4 + (pr & 3)
    pick = (pc == want).astype(F32).astype(BF)
    ur = lax.broadcasted_iota(I32, (256, 128), 0)
    uc = lax.broadcasted_iota(I32, (256, 128), 1)
    spread = [
        (((ur >> 3) == (uc >> 2)) & ((ur & 3) == (uc & 3)) & (((ur >> 2) & 1) == j))
        .astype(F32).astype(BF)
        for j in (0, 1)
    ]
    for n in range(CHUNKS):
        lo = 1 if n == 0 else 0
        chunk_refs(CHUNK * n + lo, CHUNK - lo, n, send, recv, ds, dr).wait_recv()
        block = recv[CHUNK * n : CHUNK * n + CHUNK].reshape(CHUNK * 16, 1024)
        picked = dot(pick, block).astype(BF)
        acts = []
        for j in (0, 1):
            rows = jnp.concatenate(
                [picked[256 * j : 256 * j + 128], picked[256 * j + 128 : 256 * j + 256]], axis=1
            )
            act = (silu(dot(rows, wg_s[j])) * dot(rows, wu_s[j])).astype(BF)
            acts.append(dot(spread[j], act).astype(BF))
        both = jnp.concatenate(acts, axis=1)
        done = dot(both, wd_s[...].reshape(1024, 2048))
        packed = jnp.concatenate(
            [done[:, 0:1024].reshape(CHUNK, 8, 1024), done[:, 1024:2048].reshape(CHUNK, 8, 1024)],
            axis=1,
        ).astype(BF)
        ret[CHUNK * n : CHUNK * n + CHUNK] = packed
        if n == 0:
            back[0] = packed[0]
        start_range(ret_copy, CHUNK * n + lo, CHUNK * n + CHUNK)

    for n in range(CHUNKS):
        lo = 1 if n == 0 else 0
        chunk_refs(CHUNK * n + lo, CHUNK - lo, n, ret, back, es, er).wait_recv()
        block = back[CHUNK * n : CHUNK * n + CHUNK].reshape(CHUNK * 16, 1024)
        part = dot(cw_s[:, 512 * n : 512 * n + 512], block)
        if n == 0:
            acc_s[...] = part
        else:
            acc_s[...] += part
    for h in (0, 1):
        cs = slice(1024 * h, 1024 * h + 1024)
        out_ref[:, cs] = (
            mid_s[:, cs].astype(F32) + acc_s[128 * h : 128 * h + 128, :] + shared_s[:, cs]
        ).astype(BF)
    for n in range(CHUNKS):
        lo = 1 if n == 0 else 0
        chunk_refs(CHUNK * n + lo, CHUNK - lo, n, send, recv, ds, dr).wait_send()
        chunk_refs(CHUNK * n + lo, CHUNK - lo, n, ret, back, es, er).wait_send()


def on_device(
    queries, key_matrix, value_matrix, channel_decay_input, head_decay_offset, output_gate_input,
    head_norm_gain, residual, mixer_output_weight, expert_norm_gain, routes, chosen_router_scores,
    routed_gate_weight, routed_up_weight, routed_down_weight, common_gate_weight,
    common_up_weight, common_down_weight,
):
    any_ = pl.BlockSpec(memory_space=pl.ANY)
    vm = pl.BlockSpec(memory_space=pltpu.VMEM)
    dma = pltpu.SemaphoreType.DMA
    V = pltpu.VMEM
    return pl.pallas_call(
        kernel,
        out_shape=jax.ShapeDtypeStruct((128, 2048), BF),
        in_specs=[
            any_, any_, any_, any_, vm, any_, vm, any_, any_, vm,
            vm, vm, any_, any_, any_, any_, any_, any_,
        ],
        out_specs=vm,
        scratch_shapes=[
            V((512, 128), BF), V((512, 128), BF), V((512, 256), BF), V((512, 128), BF),
            V((512, 256), BF), V((128, 2048), BF), V((1024, 2048), BF),
            V((2, 2048, 512), BF), V((2, 2048, 512), BF), V((2, 512, 2048), BF),
            V((2048, 512), BF), V((2048, 512), BF), V((512, 2048), BF),
            V((144, 128), BF), V((144, 128), BF), V((NY, 144, 128), BF), V((NZ, 144, 128), BF),
            V((2, 512, 128), F32), V((512, 128), BF), V((4, 128, 256), BF), V((4, 128, 256), BF),
            V((128, 2048), BF), V((256, 1024), BF), V((128, 2048), F32),
            V((2048, 256), BF), V((256, 2048), BF),
            V((DEVS, 16, 1024), BF), V((DEVS, 16, 1024), BF),
            V((DEVS, 16, 1024), BF), V((DEVS, 16, 1024), BF),
            V((256, 1024), F32),
            dma((13,)), dma, dma, dma((4,)), dma((4,)), dma((4,)), dma((4,)), dma((4,)), dma((4,)),
            dma((CHUNKS,)), dma((CHUNKS,)), dma((CHUNKS,)), dma((CHUNKS,)),
        ],
        compiler_params=pltpu.CompilerParams(
            collective_id=0, has_side_effects=True, vmem_limit_bytes=62 * 1024 * 1024
        ),
        name="layer",
    )(
        queries, key_matrix, value_matrix, channel_decay_input, head_decay_offset,
        output_gate_input, head_norm_gain.reshape(1, 128), residual, mixer_output_weight,
        expert_norm_gain.reshape(1, 2048), routes, chosen_router_scores, routed_gate_weight,
        routed_up_weight, routed_down_weight, common_gate_weight, common_up_weight,
        common_down_weight,
    )


def solution(mesh):
    both = ("sp", "tp")
    split, rows, rep = P("sp", "tp"), P(both, None), P()
    return jax.shard_map(
        on_device,
        mesh=mesh,
        in_specs=(
            split, split, split, split, split, split, rep, rows, rep, rep, rows, rows,
            P(both, None, None), P(both, None, None), P(both, None, None), rep, rep, rep,
        ),
        out_specs=rows,
        check_vma=False,
    )
```

time: 279 us -> 125 us (0.45)
  Pallas kernels: 0 us -> 119 us
  blocking collectives: 90.9 us -> 0 us
  local copies, waits for them, and re-layouts: 73 us -> 6.23 us
  waiting for transfers between devices: 52.6 us -> 0 us
  matrix products: 33.5 us -> 0 us
  other arithmetic: 18.5 us -> 0 us
  starting transfers between devices: 9.16 us -> 0 us
    pallas_call x0 -> x1, Pallas kernels: none -> 119 us  [on_device(): pl.pallas_call(kernel, out_shape=jax.ShapeDtypeStruct((128, 2048), BF), i...]
    all_to_all x1 -> x0, blocking collectives: 66.9 us -> none  [on_device(): lax.all_to_all(outgoing, SP_TP, split_axis=0, concat_axis=0, tiled=True)]
    all_to_all x2 -> x0, waiting for transfers between devices: 52.6 us -> none  [the longest x1 50.9 us: on_device(): lax.all_to_all(produced, SP_TP, split_axis=0, concat_axis=0, tiled=True)]
    dot_general x10 -> x0, matrix products: 33.5 us -> none  [the longest x1 14.4 us: apply_experts(): jnp.einsum('secf,efh->sech', hidden, routed_down_weight, preferred_elemen...]
    all_gather x3 -> x0, blocking collectives: 24.1 us -> none  [collected_together(): both, at, found = (lax.all_gather(jnp.concatenate(lines), axis), 0, {})]
    reshape x6 -> x0, local copies, waits for them, and re-layouts: 16.2 us -> none  [the longest x1 7.19 us: on_device(): outgoing = normed_pad[source_row].reshape(devices, exp_dev, cap_slots, D)]
    gather x2 -> x0, local copies, waits for them, and re-layouts: 14 us -> none  [the longest x1 7.96 us: on_device(): gathered = flat_back[destination].reshape(tok_count, TOP_K, D)]
    convert_element_type x2 -> x0, local copies, waits for them, and re-layouts: 12.4 us -> none  [the longest x1 7.61 us: apply_experts(): return jnp.einsum('secf,efh->sech', hidden, routed_down_weight, preferred...]
  transfers between devices with their start and end apart: 2 -> 0, of which waited for: 2 -> 0; matrix products, arithmetic and copies ran while one was open for 2% -> 0% of each run, Pallas kernels for 0% -> 0%
where the time goes in v1:
time: 125 us
  Pallas kernels  119 us (95%)
  local copies, waits for them, and re-layouts  6.23 us (5%)
    pallas_call x1, Pallas kernels, on_device(): pl.pallas_call(kernel, out_shape=jax.ShapeDtypeStruct((128, 2048), BF), i...  119 us
    unnamed x4, local copies, waits for them, and re-layouts  6.23 us

profile of v1, /device:TPU:1, one launch (start us, length us, event | category | flops | bytes accessed | tf_op | source)
XLA Modules:
  0.0 125.2 jit_solution(5036051850199853335)
XLA Ops:
  0.0 1.4 %copy.20.routes_ref = s32[128,4]{1,0:T(8,128)} copy(s32[128,4]{0,1:T(4,128)} %param.28) | data formatting | bytes 4096 | tf_op args[10]
  1.4 1.4 %copy.21.scores_ref = f32[128,4]{1,0:T(8,128)} copy(f32[128,4]{0,1:T(4,128)} %param.29) | data formatting | bytes 4096 | tf_op args[11]
  2.8 1.5 %copy.19.hd_ref = f32[512,2]{1,0:T(8,128)} copy(f32[512,2]{0,1:T(2,128)} %param.22) | data formatting | bytes 8192 | tf_op args[4]
  4.4 119.0 %layer.1 = bf16[128,2048]{1,0:T(8,128)(2,1)} custom-call(bf16[512,128]{1,0:T(8,128)(2,1)} %q_hbm.1, bf16[512,128]{1,0:T(8,128)(2,1)} %k_hbm.1, bf16[512,256]{1,0:T(8,128)(2,1)} %v_hbm.1, bf16[512,128]{1,0:T(8,128)(2,1)} %cd_hbm.1, f32[512,2]{1,0:T(8,128)} %copy.19.hd_ref, bf16[512,256]{1,0:T(8,128)(2,1)} %og_hbm.1, f32[1,128]{1,0:T(1,128)} %bitcast.3, ...), custom_call_target="tpu_custom_call" | custom-call | tf_op jit(solution)/shard_map/layer/pallas_call | solution.py:414
  123.3 1.9 %copy.23 = bf16[128,2048]{1,0:T(8,128)(2,1)} copy(bf16[128,2048]{1,0:T(8,128)(2,1)} %layer.1) | data formatting | bytes 1048576

commit v2 on v1

--- a/solution.py
+++ b/solution.py
@@ -74,7 +74,7 @@
             )
         )
     ]
-    for one in loads:
+    for one in loads[:5]:
         one.start()
     (l_cd, l_k, l_v, l_q, l_og, l_wo, l_res, l_cg, l_cu, l_cdn, l_wg, l_wu, l_wd) = loads
 
@@ -92,7 +92,8 @@
     cols_i = lax.broadcasted_iota(I32, (256, 256), 1)
     causal = (rows_i >= cols_i) & ((rows_i >> 6) == (cols_i >> 6))
     tri = causal.astype(F32).astype(BF)
-    hd = jnp.where(first, hd_ref[:, 0:1], hd_ref[:, 1:2])
+    hd_t = jnp.concatenate([hd_ref[...], jnp.zeros((6, 512), F32)], axis=0).T
+    hd = jnp.where(first, hd_t[:, 0:1], hd_t[:, 1:2])
     l_cd.wait()
     cd = cd_s[...].astype(F32)
     dl = (jnp.minimum(cd, 0.0) - jnp.log1p(jnp.exp(-jnp.abs(cd)))) / RUNNING + hd
@@ -138,6 +139,8 @@
         device_id=place(z, y, c + 1, x), device_id_type=MESH,
     )
     core_copy.start()
+    for one in loads[5:]:
+        one.start()
 
     l_q.wait()
     ew = jnp.exp(within)
@@ -216,15 +219,12 @@
         dev = ((z + (off >> 5)) & 3) * 8 + ((y + (off >> 3)) & 3) * 2 + ((c + off) & 1)
         return (dev * 4 + ((x + (off >> 1)) & 3)) * 2 + ((index >> 2) & 1)
 
-    routes = routes_ref[...].astype(F32)
+    turned = routes_ref[...].astype(F32)
+    routes = jnp.concatenate([turned, jnp.zeros((124, 128), F32)], axis=0).T
     sub128 = lax.broadcasted_iota(I32, (128, 128), 0)
     lan128 = lax.broadcasted_iota(I32, (128, 128), 1)
     upper = (sub128 < lan128).astype(F32).astype(BF)
     lower = (sub128 > lan128).astype(F32).astype(BF)
-    wide = jnp.zeros((128, 128), F32)
-    for n in range(4):
-        wide = jnp.where(lan128 == n, routes[:, n : n + 1], wide)
-    turned = wide.T
     for n in range(8):
         q_index = lax.broadcasted_iota(I32, (256, 128), 0) + 256 * n
         expert = expert_of(q_index).astype(F32)
@@ -237,7 +237,8 @@
         lhs_s[256 * n : 256 * n + 256, 0:128] = jnp.where(half, live, 0.0).astype(BF)
         lhs_s[256 * n : 256 * n + 256, 128:256] = jnp.where(half, 0.0, live).astype(BF)
     scores = scores_ref[...]
-    weights = SCALE * scores / jnp.sum(scores, axis=-1, keepdims=True)
+    weights = SCALE * scores / jnp.sum(scores, axis=0, keepdims=True)
+    weights = jnp.concatenate([weights, jnp.zeros((124, 128), F32)], axis=0).T
     for n in range(4):
         q_index = lax.broadcasted_iota(I32, (128, 512), 1) + 512 * n
         expert = expert_of(q_index).astype(F32)
@@ -439,9 +440,9 @@
         ),
         name="layer",
     )(
-        queries, key_matrix, value_matrix, channel_decay_input, head_decay_offset,
+        queries, key_matrix, value_matrix, channel_decay_input, head_decay_offset.T,
         output_gate_input, head_norm_gain.reshape(1, 128), residual, mixer_output_weight,
-        expert_norm_gain.reshape(1, 2048), routes, chosen_router_scores, routed_gate_weight,
+        expert_norm_gain.reshape(1, 2048), routes.T, chosen_router_scores.T, routed_gate_weight,
         routed_up_weight, routed_down_weight, common_gate_weight, common_up_weight,
         common_down_weight,
     )

time: 125 us -> 121 us (0.968)
  local copies, waits for them, and re-layouts: 6.23 us -> 1.88 us
    unnamed x4 -> x1, local copies, waits for them, and re-layouts: 6.23 us -> 1.88 us
where the time goes in v2:
time: 121 us; the launch traced here: 120 us
  Pallas kernels  118 us (98%)
  local copies, waits for them, and re-layouts  1.88 us (2%)
    pallas_call x1, Pallas kernels, on_device(): pl.pallas_call(kernel, out_shape=jax.ShapeDtypeStruct((128, 2048), BF), i...  118 us

profile of v2, /device:TPU:1, one launch (start us, length us, event | category | flops | bytes accessed | tf_op | source)
XLA Modules:
  0.0 120.3 jit_solution(12286437619597033559)
XLA Ops:
  0.0 118.4 %layer.1 = bf16[128,2048]{1,0:T(8,128)(2,1)} custom-call(bf16[512,128]{1,0:T(8,128)(2,1)} %q_hbm.1, bf16[512,128]{1,0:T(8,128)(2,1)} %k_hbm.1, bf16[512,256]{1,0:T(8,128)(2,1)} %v_hbm.1, bf16[512,128]{1,0:T(8,128)(2,1)} %cd_hbm.1, f32[2,512]{1,0:T(2,128)} %bitcast.6, bf16[512,256]{1,0:T(8,128)(2,1)} %og_hbm.1, f32[1,128]{1,0:T(1,128)} %bitcast.9, ...), custom_call_target="tpu_custom_call" | custom-call | tf_op jit(solution)/shard_map/layer/pallas_call | solution.py:415
  118.4 1.9 %copy.20 = bf16[128,2048]{1,0:T(8,128)(2,1)} copy(bf16[128,2048]{1,0:T(8,128)(2,1)} %layer.1) | data formatting | bytes 1048576

commit v3 on v2

--- a/solution.py
+++ b/solution.py
@@ -13,9 +13,10 @@
 BLOCK = 64
 NZ, NY, NC, NX = 4, 4, 2, 4
 DEVS = NZ * NY * NC * NX
-STRIDE = 37
-CHUNK = 32
-CHUNKS = DEVS // CHUNK
+STEP = 5
+WIDTHS = (640, 640, 768)
+STARTS = (0, 640, 1280)
+AXES = (0, 1, 2)
 
 EPS = 1e-6
 RUNNING = 16.0
@@ -51,9 +52,11 @@
     routes_ref, scores_ref, wg_hbm, wu_hbm, wd_hbm, cg_hbm, cu_hbm, cdn_hbm,
     out_ref,
     q_s, k_s, v_s, cd_s, og_s, res_s, wo_s, wg_s, wu_s, wd_s, cg_s, cu_s, cdn_s,
-    st1, st1r, st2, st3, outacc, qx_s, gsend, grecv, mid_s, nrm_s, shared_s,
-    lhs_s, cw_s, send, recv, ret, back, acc_s,
-    load_sem, s1, r1, s2, r2, s3, r3, gs, gr, ds, dr, es, er,
+    st1, st1r, st2, st3, outacc, qx_s, gsend, grecv, mid_s, shared_s,
+    rt_s, lhs_s, cw_s, pick_s, place_s,
+    bx, by, bz, px, py, pz, sx, sy, sz, rx, ry, rz, tx, ty, tz, kx, ky, kz,
+    load_sem, s1, r1, s2, r2, s3, r3, gs, gr,
+    ts, tr, bs, br, ds, dr, es, er, ps, pr,
 ):
     sp = lax.axis_index("sp")
     x = lax.axis_index("tp")
@@ -63,6 +66,38 @@
 
     def place(zz, yy, cc, xx):
         return ((zz % NZ) * (NY * NC) + (yy % NY) * NC + cc % NC, xx % NX)
+
+    lines, sums = (bx, by, bz), (px, py, pz)
+    send, recv, ret, back = (sx, sy, sz), (rx, ry, rz), (tx, ty, tz), (kx, ky, kz)
+
+    def along(a, d):
+        return place(z + (d if a == 2 else 0), y + (d if a == 1 else 0), c, x + (d if a == 0 else 0))
+
+    def across(a, n, i, sign):
+        k = (i * STEP) % 16
+        d1, d2, dc = sign * (k // 4), sign * (k % 4), sign * n
+        if a == 0:
+            return place(z + NZ + d1, y + NY + d2, c + NC + dc, x)
+        if a == 1:
+            return place(z + NZ + d1, y, c + NC + dc, x + NX + d2)
+        return place(z, y + NY + d1, c + NC + dc, x + NX + d2)
+
+    def plane_split(i):
+        k = (i * STEP) & 15
+        return k >> 2, k & 3
+
+    def expert_of(a, n, i, j):
+        d1, d2 = plane_split(i)
+        zz = (z + (0 if a == 2 else d1)) & 3
+        yy = (y + (0 if a == 1 else (d2 if a == 0 else d1))) & 3
+        xx = (x + (0 if a == 0 else d2)) & 3
+        return ((zz * 8 + yy * 2 + ((c + n) & 1)) * 4 + xx) * 2 + j
+
+    def line_copy(a, d, src, dst, ssem, rsem, sign):
+        return pltpu.make_async_remote_copy(
+            src_ref=src, dst_ref=dst, send_sem=ssem.at[4 * a + d], recv_sem=rsem.at[4 * a + d],
+            device_id=along(a, d if sign > 0 else 4 - d), device_id_type=MESH,
+        )
 
     loads = [
         pltpu.make_async_copy(a, b, load_sem.at[n])
@@ -133,12 +168,20 @@
         return log, ref[0:128, :].astype(F32)
 
     put_state(st1, total, own_state)
+    scores = scores_ref[...]
+    weights = SCALE * scores / jnp.sum(scores, axis=0, keepdims=True)
+    rt_s[0] = jnp.concatenate([routes_ref[...].astype(F32), weights], axis=0)
     pl.semaphore_wait(bar, 10)
     core_copy = pltpu.make_async_remote_copy(
         src_ref=st1, dst_ref=st1r, send_sem=s1, recv_sem=r1,
         device_id=place(z, y, c + 1, x), device_id_type=MESH,
     )
     core_copy.start()
+    rt_copies = [
+        line_copy(a, d, rt_s.at[0], rt_s.at[4 * a + d], ts, tr, 1) for a in AXES for d in (1, 2, 3)
+    ]
+    for one in rt_copies:
+        one.start()
     for one in loads[5:]:
         one.start()
 
@@ -214,45 +257,28 @@
     plane_log, plane_state, carry_log, carry_state = prefix(st2, y, NY, carry_log, carry_state)
     z_copies = exchange(st3, z, plane_log, plane_state, s3, r3, lambda d: place(z + d, y, c, x))
 
-    def expert_of(index):
-        off = ((index >> 4) * STRIDE) & (DEVS - 1)
-        dev = ((z + (off >> 5)) & 3) * 8 + ((y + (off >> 3)) & 3) * 2 + ((c + off) & 1)
-        return (dev * 4 + ((x + (off >> 1)) & 3)) * 2 + ((index >> 2) & 1)
-
-    turned = routes_ref[...].astype(F32)
-    routes = jnp.concatenate([turned, jnp.zeros((124, 128), F32)], axis=0).T
+    for one in rt_copies:
+        one.wait()
     sub128 = lax.broadcasted_iota(I32, (128, 128), 0)
     lan128 = lax.broadcasted_iota(I32, (128, 128), 1)
     upper = (sub128 < lan128).astype(F32).astype(BF)
     lower = (sub128 > lan128).astype(F32).astype(BF)
-    for n in range(8):
-        q_index = lax.broadcasted_iota(I32, (256, 128), 0) + 256 * n
-        expert = expert_of(q_index).astype(F32)
-        match = jnp.zeros((256, 128), F32)
-        for j in range(4):
-            match = jnp.where(expert == turned[j : j + 1, :], 1.0, match)
-        rank = dot(match.astype(BF), upper)
-        live = jnp.where(rank == (q_index & 3).astype(F32), match, 0.0)
-        half = ((q_index >> 3) & 1) == 0
-        lhs_s[256 * n : 256 * n + 256, 0:128] = jnp.where(half, live, 0.0).astype(BF)
-        lhs_s[256 * n : 256 * n + 256, 128:256] = jnp.where(half, 0.0, live).astype(BF)
-    scores = scores_ref[...]
-    weights = SCALE * scores / jnp.sum(scores, axis=0, keepdims=True)
-    weights = jnp.concatenate([weights, jnp.zeros((124, 128), F32)], axis=0).T
-    for n in range(4):
-        q_index = lax.broadcasted_iota(I32, (128, 512), 1) + 512 * n
-        expert = expert_of(q_index).astype(F32)
-        weight = jnp.zeros((128, 512), F32)
-        match = jnp.zeros((128, 512), F32)
-        for j in range(4):
-            hit = expert == routes[:, j : j + 1]
-            match = jnp.where(hit, 1.0, match)
-            weight = jnp.where(hit, weights[:, j : j + 1], weight)
-        rank = dot(lower, match.astype(BF))
-        weight = jnp.where(rank == (q_index & 3).astype(F32), weight, 0.0)
-        half = ((q_index >> 3) & 1) == 0
-        cw_s[0:128, 512 * n : 512 * n + 512] = jnp.where(half, weight, 0.0).astype(BF)
-        cw_s[128:256, 512 * n : 512 * n + 512] = jnp.where(half, 0.0, weight).astype(BF)
+    nothing = jnp.zeros((32, 8, 128), F32)
+    q_index = lax.broadcasted_iota(I32, (256, 128), 0)
+    for a in AXES:
+        expert = expert_of(a, q_index >> 7, (q_index >> 3) & 15, (q_index >> 2) & 1).astype(F32)
+        for d in range(4):
+            info = rt_s[4 * a + d if d else 0]
+            match = jnp.zeros((256, 128), F32)
+            for j in range(4):
+                match = jnp.where(expert == info[j : j + 1, :], 1.0, match)
+            rank = dot(match.astype(BF), upper)
+            live = jnp.where(rank == (q_index & 3).astype(F32), match, 0.0).reshape(32, 8, 128)
+            pair = [live, nothing] if d % 2 == 0 else [nothing, live]
+            cols = slice(128 * (d % 2), 128 * (d % 2) + 128)
+            lhs_s[2 * a + d // 2, :, cols] = (
+                jnp.concatenate(pair, axis=1).reshape(512, 128).astype(BF)
+            )
 
     for one in z_copies:
         one.wait()
@@ -293,113 +319,151 @@
     mid_w = middle.astype(F32)
     scale = lax.rsqrt(jnp.mean(mid_w * mid_w, axis=-1, keepdims=True) + EPS)
     normed = (mid_w * scale * egain_ref[...]).astype(BF)
-    nrm_s[0:128, :] = normed[:, 0:1024]
-    nrm_s[128:256, :] = normed[:, 1024:2048]
-
-    def target(i, sign):
-        k = (i * STRIDE) % DEVS
-        return place(
-            z + NZ + sign * (k // 32), y + NY + sign * ((k // 8) % 4),
-            c + NC + sign * (k % 2), x + NX + sign * ((k // 2) % 4),
+    b_copies = {}
+    for a in AXES:
+        lines[a][0] = normed[:, STARTS[a] : STARTS[a] + WIDTHS[a]]
+        for d in (1, 2, 3):
+            b_copies[a, d] = line_copy(a, d, lines[a].at[0], lines[a].at[d], bs, br, 1)
+    for d in (1, 3, 2):
+        for a in AXES:
+            b_copies[a, d].start()
+
+    def sem(a, half, n):
+        return 4 * a + 2 * half + n
+
+    def plane_copies(half, n, source, dest, ssem, rsem, sign):
+        def body(i, carry):
+            for a in AXES:
+                pltpu.make_async_remote_copy(
+                    src_ref=source[a].at[n, half, i], dst_ref=dest[a].at[n, half, i],
+                    send_sem=ssem.at[sem(a, half, n)], recv_sem=rsem.at[sem(a, half, n)],
+                    device_id=across(a, n, i, sign), device_id_type=MESH,
+                ).start()
+            return carry
+
+        lax.fori_loop(1 if n == 0 else 0, 16, body, 0)
+
+    def plane_wait(a, half, n, source, dest, ssem, rsem):
+        part = pl.ds(1, 15) if n == 0 else pl.ds(0, 16)
+        return pltpu.make_async_remote_copy(
+            src_ref=source[a].at[n, half, part], dst_ref=dest[a].at[n, half, part],
+            send_sem=ssem.at[sem(a, half, n)], recv_sem=rsem.at[sem(a, half, n)],
+            device_id=across(a, 1, 1, 1), device_id_type=MESH,
         )
 
-    def send_copy(i):
-        return pltpu.make_async_remote_copy(
-            src_ref=send.at[i], dst_ref=recv.at[i],
-            send_sem=ds.at[i // CHUNK], recv_sem=dr.at[i // CHUNK],
-            device_id=target(i, 1), device_id_type=MESH,
-        )
-
-    def ret_copy(i):
-        return pltpu.make_async_remote_copy(
-            src_ref=ret.at[i], dst_ref=back.at[i],
-            send_sem=es.at[i // CHUNK], recv_sem=er.at[i // CHUNK],
-            device_id=target(i, -1), device_id_type=MESH,
-        )
-
-    def chunk_refs(first_slot, count, n, a, b, asem, bsem):
-        return pltpu.make_async_remote_copy(
-            src_ref=a.at[pl.ds(first_slot, count)], dst_ref=b.at[pl.ds(first_slot, count)],
-            send_sem=asem.at[n], recv_sem=bsem.at[n],
-            device_id=target(1, 1), device_id_type=MESH,
-        )
-
-    def start_range(make, lo, hi):
-        def body(i, carry):
-            make(i).start()
-            return carry
-
-        lax.fori_loop(lo, hi, body, 0)
-
-    for n in range(8):
-        rows = dot(lhs_s[256 * n : 256 * n + 256, :], nrm_s[...]).astype(BF).reshape(16, 16, 1024)
-        send[16 * n : 16 * n + 16] = rows
-        if n == 0:
-            recv[0] = rows[0]
-        start_range(send_copy, max(16 * n, 1), 16 * n + 16)
+    for n in (0, 1):
+        for half in (0, 1):
+            for a in AXES:
+                if n == 0:
+                    for d in (1,) if half == 0 else (3, 2):
+                        b_copies[a, d].wait_recv()
+                rows = dot(
+                    lhs_s[2 * a + half, 256 * n : 256 * n + 256, :],
+                    lines[a][2 * half : 2 * half + 2].reshape(256, WIDTHS[a]),
+                ).astype(BF).reshape(16, 16, WIDTHS[a])
+                send[a][n, half] = rows
+                if n == 0:
+                    recv[a][0, half, 0] = rows[0]
+            plane_copies(half, n, send, recv, ds, dr, 1)
 
     l_cg.wait()
     l_cu.wait()
     l_cdn.wait()
-    nrm = jnp.concatenate([nrm_s[0:128, :], nrm_s[128:256, :]], axis=1)
+    nrm = jnp.concatenate([lines[a][0] for a in AXES], axis=1)
     hidden = (silu(dot(nrm, cg_s[...])) * dot(nrm, cu_s[...])).astype(BF)
     shared_s[...] = dot(hidden, cdn_s[...])
+
+    def row_of(a, q):
+        d1, d2 = plane_split((q >> 4) & 15)
+        d = ((q >> 8) & 1) * 2 + ((q >> 3) & 1)
+        dz, dy, dx = ((d1, d2, d), (d1, d, d2), (d, d1, d2))[a]
+        return ((q >> 2) & 1) * 256 + (dz * 16 + dy * 4 + dx) * 4 + (q & 3)
+
+    down = lax.broadcasted_iota(I32, (512, 512), 0)
+    over = lax.broadcasted_iota(I32, (512, 512), 1)
+    for a in AXES:
+        pick_s[a] = (down == row_of(a, over)).astype(F32).astype(BF)
+        place_s[a] = (over == row_of(a, down)).astype(F32).astype(BF)
+    q_index = lax.broadcasted_iota(I32, (128, 512), 1)
+    blank = jnp.zeros((120, 128), F32)
+    for a in AXES:
+        expert = expert_of(a, q_index >> 8, (q_index >> 4) & 15, (q_index >> 2) & 1).astype(F32)
+        for d in range(4):
+            info = jnp.concatenate([rt_s[4 * a + d if d else 0], blank], axis=0).T
+            weight = jnp.zeros((128, 512), F32)
+            match = jnp.zeros((128, 512), F32)
+            for j in range(4):
+                hit = expert == info[:, j : j + 1]
+                match = jnp.where(hit, 1.0, match)
+                weight = jnp.where(hit, info[:, 4 + j : 5 + j], weight)
+            rank = dot(lower, match.astype(BF))
+            live = (rank == (q_index & 3).astype(F32)) & (((q_index >> 3) & 1) == d % 2)
+            rows = slice(128 * (d % 2), 128 * (d % 2) + 128)
+            cw_s[2 * a + d // 2, rows, :] = jnp.where(live, weight, 0.0).astype(BF)
 
     l_wg.wait()
     l_wu.wait()
     l_wd.wait()
-    pr = lax.broadcasted_iota(I32, (512, 512), 0)
-    pc = lax.broadcasted_iota(I32, (512, 512), 1)
-    want = ((pr >> 2) & 31) * 16 + ((pr >> 7) & 1) * 8 + (pr >> 8) * 4 + (pr & 3)
-    pick = (pc == want).astype(F32).astype(BF)
-    ur = lax.broadcasted_iota(I32, (256, 128), 0)
-    uc = lax.broadcasted_iota(I32, (256, 128), 1)
-    spread = [
-        (((ur >> 3) == (uc >> 2)) & ((ur & 3) == (uc & 3)) & (((ur >> 2) & 1) == j))
-        .astype(F32).astype(BF)
-        for j in (0, 1)
-    ]
-    for n in range(CHUNKS):
-        lo = 1 if n == 0 else 0
-        chunk_refs(CHUNK * n + lo, CHUNK - lo, n, send, recv, ds, dr).wait_recv()
-        block = recv[CHUNK * n : CHUNK * n + CHUNK].reshape(CHUNK * 16, 1024)
-        picked = dot(pick, block).astype(BF)
+    for n in (0, 1):
+        picked = []
+        for a in AXES:
+            for half in (0, 1):
+                plane_wait(a, half, n, send, recv, ds, dr).wait_recv()
+            picked.append(dot(pick_s[a], recv[a][n].reshape(512, WIDTHS[a])).astype(BF))
         acts = []
         for j in (0, 1):
-            rows = jnp.concatenate(
-                [picked[256 * j : 256 * j + 128], picked[256 * j + 128 : 256 * j + 256]], axis=1
-            )
-            act = (silu(dot(rows, wg_s[j])) * dot(rows, wu_s[j])).astype(BF)
-            acts.append(dot(spread[j], act).astype(BF))
-        both = jnp.concatenate(acts, axis=1)
-        done = dot(both, wd_s[...].reshape(1024, 2048))
-        packed = jnp.concatenate(
-            [done[:, 0:1024].reshape(CHUNK, 8, 1024), done[:, 1024:2048].reshape(CHUNK, 8, 1024)],
-            axis=1,
-        ).astype(BF)
-        ret[CHUNK * n : CHUNK * n + CHUNK] = packed
-        if n == 0:
-            back[0] = packed[0]
-        start_range(ret_copy, CHUNK * n + lo, CHUNK * n + CHUNK)
-
-    for n in range(CHUNKS):
-        lo = 1 if n == 0 else 0
-        chunk_refs(CHUNK * n + lo, CHUNK - lo, n, ret, back, es, er).wait_recv()
-        block = back[CHUNK * n : CHUNK * n + CHUNK].reshape(CHUNK * 16, 1024)
-        part = dot(cw_s[:, 512 * n : 512 * n + 512], block)
-        if n == 0:
-            acc_s[...] = part
-        else:
-            acc_s[...] += part
-    for h in (0, 1):
-        cs = slice(1024 * h, 1024 * h + 1024)
-        out_ref[:, cs] = (
-            mid_s[:, cs].astype(F32) + acc_s[128 * h : 128 * h + 128, :] + shared_s[:, cs]
-        ).astype(BF)
-    for n in range(CHUNKS):
-        lo = 1 if n == 0 else 0
-        chunk_refs(CHUNK * n + lo, CHUNK - lo, n, send, recv, ds, dr).wait_send()
-        chunk_refs(CHUNK * n + lo, CHUNK - lo, n, ret, back, es, er).wait_send()
+            rows = jnp.concatenate([p[256 * j : 256 * j + 256] for p in picked], axis=1)
+            acts.append((silu(dot(rows, wg_s[j])) * dot(rows, wu_s[j])).astype(BF))
+        for half in (1, 0):
+            for a in AXES:
+                rows = slice(256 * half, 256 * half + 256)
+                both = jnp.concatenate(
+                    [dot(place_s[a, rows, 256 * j : 256 * j + 256], acts[j]).astype(BF) for j in (0, 1)],
+                    axis=1,
+                )
+                cols = slice(STARTS[a], STARTS[a] + WIDTHS[a])
+                done = jnp.concatenate([wd_s[0, :, cols], wd_s[1, :, cols]], axis=0)
+                done = dot(both, done).astype(BF).reshape(16, 16, WIDTHS[a])
+                ret[a][n, half] = done
+                if n == 0:
+                    back[a][0, half, 0] = done[0]
+            plane_copies(half, n, ret, back, es, er, -1)
+
+    for one in b_copies.values():
+        one.wait_send()
+    p_copies = []
+    for half in (1, 0):
+        for a in AXES:
+            total_a = jnp.zeros((256, WIDTHS[a]), F32)
+            for n in (0, 1):
+                plane_wait(a, half, n, ret, back, es, er).wait_recv()
+                total_a = total_a + dot(
+                    cw_s[2 * a + half, :, 256 * n : 256 * n + 256],
+                    back[a][n, half].reshape(256, WIDTHS[a]),
+                )
+            for d in (2 * half, 2 * half + 1):
+                mine = total_a[128 * (d % 2) : 128 * (d % 2) + 128]
+                if d == 0:
+                    cols = slice(STARTS[a], STARTS[a] + WIDTHS[a])
+                    shared_s[:, cols] += mine
+                else:
+                    lines[a][d] = mine.astype(BF)
+                    one = line_copy(a, d, lines[a].at[d], sums[a].at[d - 1], ps, pr, -1)
+                    one.start()
+                    p_copies.append(one)
+    for one in p_copies:
+        one.wait()
+    for a in AXES:
+        cols = slice(STARTS[a], STARTS[a] + WIDTHS[a])
+        value = mid_s[:, cols].astype(F32) + shared_s[:, cols]
+        for d in range(3):
+            value = value + sums[a][d].astype(F32)
+        out_ref[:, cols] = value.astype(BF)
+    for n in (0, 1):
+        for half in (0, 1):
+            for a in AXES:
+                plane_wait(a, half, n, send, recv, ds, dr).wait_send()
+                plane_wait(a, half, n, ret, back, es, er).wait_send()
 
 
 def on_device(
@@ -427,13 +491,13 @@
             V((2048, 512), BF), V((2048, 512), BF), V((512, 2048), BF),
             V((144, 128), BF), V((144, 128), BF), V((NY, 144, 128), BF), V((NZ, 144, 128), BF),
             V((2, 512, 128), F32), V((512, 128), BF), V((4, 128, 256), BF), V((4, 128, 256), BF),
-            V((128, 2048), BF), V((256, 1024), BF), V((128, 2048), F32),
-            V((2048, 256), BF), V((256, 2048), BF),
-            V((DEVS, 16, 1024), BF), V((DEVS, 16, 1024), BF),
-            V((DEVS, 16, 1024), BF), V((DEVS, 16, 1024), BF),
-            V((256, 1024), F32),
+            V((128, 2048), BF), V((128, 2048), F32),
+            V((12, 8, 128), F32), V((6, 512, 256), BF), V((6, 256, 512), BF),
+            V((3, 512, 512), BF), V((3, 512, 512), BF),
+            *[V((4, 128, w), BF) for w in WIDTHS], *[V((3, 128, w), BF) for w in WIDTHS],
+            *[V((2, 2, 16, 16, w), BF) for _ in range(4) for w in WIDTHS],
             dma((13,)), dma, dma, dma((4,)), dma((4,)), dma((4,)), dma((4,)), dma((4,)), dma((4,)),
-            dma((CHUNKS,)), dma((CHUNKS,)), dma((CHUNKS,)), dma((CHUNKS,)),
+            *[dma((12,)) for _ in range(10)],
         ],
         compiler_params=pltpu.CompilerParams(
             collective_id=0, has_side_effects=True, vmem_limit_bytes=62 * 1024 * 1024

time: 121 us -> 107 us (0.88)
  Pallas kernels: 118 us -> 105 us
    pallas_call x1, Pallas kernels: 118 us -> 105 us  [on_device(): pl.pallas_call(kernel, out_shape=jax.ShapeDtypeStruct((128, 2048), BF), i...]
where the time goes in v3:
time: 107 us
  Pallas kernels  105 us (98%)
  local copies, waits for them, and re-layouts  1.88 us (2%)
    pallas_call x1, Pallas kernels, on_device(): pl.pallas_call(kernel, out_shape=jax.ShapeDtypeStruct((128, 2048), BF), i...  105 us

profile of v3, /device:TPU:1, one launch (start us, length us, event | category | flops | bytes accessed | tf_op | source)
XLA Modules:
  0.0 106.6 jit_solution(10792932617271966169)
XLA Ops:
  0.0 104.7 %layer.1 = bf16[128,2048]{1,0:T(8,128)(2,1)} custom-call(bf16[512,128]{1,0:T(8,128)(2,1)} %q_hbm.1, bf16[512,128]{1,0:T(8,128)(2,1)} %k_hbm.1, bf16[512,256]{1,0:T(8,128)(2,1)} %v_hbm.1, bf16[512,128]{1,0:T(8,128)(2,1)} %cd_hbm.1, f32[2,512]{1,0:T(2,128)} %bitcast.6, bf16[512,256]{1,0:T(8,128)(2,1)} %og_hbm.1, f32[1,128]{1,0:T(1,128)} %bitcast.9, ...), custom_call_target="tpu_custom_call" | custom-call | tf_op jit(solution)/shard_map/layer/pallas_call | solution.py:479
  104.7 1.9 %copy.20 = bf16[128,2048]{1,0:T(8,128)(2,1)} copy(bf16[128,2048]{1,0:T(8,128)(2,1)} %layer.1) | data formatting | bytes 1048576

commit v4 on v3

--- a/solution.py
+++ b/solution.py
@@ -16,6 +16,7 @@
 STEP = 5
 WIDTHS = (640, 640, 768)
 STARTS = (0, 640, 1280)
+FIRST = (384, 384, 384)
 AXES = (0, 1, 2)
 
 EPS = 1e-6
@@ -52,7 +53,7 @@
     routes_ref, scores_ref, wg_hbm, wu_hbm, wd_hbm, cg_hbm, cu_hbm, cdn_hbm,
     out_ref,
     q_s, k_s, v_s, cd_s, og_s, res_s, wo_s, wg_s, wu_s, wd_s, cg_s, cu_s, cdn_s,
-    st1, st1r, st2, st3, outacc, qx_s, gsend, grecv, mid_s, shared_s,
+    st1, st1r, st2, st3, outacc, qx_s, gsend, grecv, mid_s, shared_s, third_s,
     rt_s, lhs_s, cw_s, pick_s, place_s,
     bx, by, bz, px, py, pz, sx, sy, sz, rx, ry, rz, tx, ty, tz, kx, ky, kz,
     load_sem, s1, r1, s2, r2, s3, r3, gs, gr,
@@ -319,14 +320,34 @@
     mid_w = middle.astype(F32)
     scale = lax.rsqrt(jnp.mean(mid_w * mid_w, axis=-1, keepdims=True) + EPS)
     normed = (mid_w * scale * egain_ref[...]).astype(BF)
+    def columns(a, part):
+        return slice(0, FIRST[a]) if part == 0 else slice(FIRST[a], WIDTHS[a])
+
+    def relay(a, part, source, dest, ssem, rsem, toward):
+        cols = columns(a, part)
+        return pltpu.make_async_remote_copy(
+            src_ref=source.at[:, cols], dst_ref=dest.at[:, cols],
+            send_sem=ssem, recv_sem=rsem,
+            device_id=along(a, toward), device_id_type=MESH,
+        )
+
     b_copies = {}
     for a in AXES:
         lines[a][0] = normed[:, STARTS[a] : STARTS[a] + WIDTHS[a]]
-        for d in (1, 2, 3):
-            b_copies[a, d] = line_copy(a, d, lines[a].at[0], lines[a].at[d], bs, br, 1)
-    for d in (1, 3, 2):
-        for a in AXES:
-            b_copies[a, d].start()
+        for part in (0, 1):
+            for d in (1, 3):
+                n = 8 * a + 2 * part + d // 2
+                b_copies[a, d, part] = relay(
+                    a, part, lines[a].at[0], lines[a].at[d], bs.at[n], br.at[n], d
+                )
+            n, d = 8 * a + 4 + part, 1 + 2 * part
+            b_copies[a, 2, part] = relay(
+                a, part, lines[a].at[d], lines[a].at[2], bs.at[n], br.at[n], d
+            )
+    for part in (0, 1):
+        for d in (1, 3):
+            for a in AXES:
+                b_copies[a, d, part].start()
 
     def sem(a, half, n):
         return 4 * a + 2 * half + n
@@ -343,6 +364,30 @@
 
         lax.fori_loop(1 if n == 0 else 0, 16, body, 0)
 
+    def split_copy(n, a, part, i, source, dest, ssem, rsem, sign):
+        at = sem(a, 0, n) if part == 0 else 12 + a
+        cols = columns(a, part)
+        return pltpu.make_async_remote_copy(
+            src_ref=source[a].at[n, 0, i, :, cols], dst_ref=dest[a].at[n, 0, i, :, cols],
+            send_sem=ssem.at[at], recv_sem=rsem.at[at],
+            device_id=across(a, 1, 1, sign) if isinstance(i, slice) else across(a, n, i, sign),
+            device_id_type=MESH,
+        )
+
+    def split_copies(n, part, source, dest, ssem, rsem, sign):
+        def body(i, carry):
+            for a in AXES:
+                split_copy(n, a, part, i, source, dest, ssem, rsem, sign).start()
+            return carry
+
+        lax.fori_loop(1 if n == 0 else 0, 16, body, 0)
+
+    def out_wait(a, part):
+        return split_copy(0, a, part, slice(1, 16), send, recv, ds, dr, 1)
+
+    def last_wait(a, part):
+        return split_copy(1, a, part, slice(0, 16), ret, back, es, er, -1)
+
     def plane_wait(a, half, n, source, dest, ssem, rsem):
         part = pl.ds(1, 15) if n == 0 else pl.ds(0, 16)
         return pltpu.make_async_remote_copy(
@@ -351,20 +396,34 @@
             device_id=across(a, 1, 1, 1), device_id_type=MESH,
         )
 
-    for n in (0, 1):
-        for half in (0, 1):
-            for a in AXES:
-                if n == 0:
-                    for d in (1,) if half == 0 else (3, 2):
-                        b_copies[a, d].wait_recv()
-                rows = dot(
-                    lhs_s[2 * a + half, 256 * n : 256 * n + 256, :],
-                    lines[a][2 * half : 2 * half + 2].reshape(256, WIDTHS[a]),
-                ).astype(BF).reshape(16, 16, WIDTHS[a])
-                send[a][n, half] = rows
-                if n == 0:
-                    recv[a][0, half, 0] = rows[0]
-            plane_copies(half, n, send, recv, ds, dr, 1)
+    for part in (0, 1):
+        for a in AXES:
+            b_copies[a, 1, part].wait_recv()
+            if part == 1:
+                b_copies[a, 3, 1].wait_recv()
+            b_copies[a, 2, part].start()
+        for a in AXES:
+            cols = columns(a, part)
+            wide = cols.stop - cols.start
+            rows = dot(lhs_s[2 * a, 0:256, :], lines[a][0:2, :, cols].reshape(256, wide))
+            rows = rows.astype(BF).reshape(16, 16, wide)
+            send[a][0, 0, :, :, cols] = rows
+            recv[a][0, 0, 0, :, cols] = rows[0]
+        split_copies(0, part, send, recv, ds, dr, 1)
+    for n, half in ((0, 1), (1, 0), (1, 1)):
+        for a in AXES:
+            if n == 0:
+                b_copies[a, 3, 0].wait_recv()
+                b_copies[a, 2, 0].wait_recv()
+                b_copies[a, 2, 1].wait_recv()
+            rows = dot(
+                lhs_s[2 * a + half, 256 * n : 256 * n + 256, :],
+                lines[a][2 * half : 2 * half + 2].reshape(256, WIDTHS[a]),
+            ).astype(BF).reshape(16, 16, WIDTHS[a])
+            send[a][n, half] = rows
+            if n == 0:
+                recv[a][0, half, 0] = rows[0]
+        plane_copies(half, n, send, recv, ds, dr, 1)
 
     l_cg.wait()
     l_cu.wait()
@@ -408,7 +467,11 @@
         picked = []
         for a in AXES:
             for half in (0, 1):
-                plane_wait(a, half, n, send, recv, ds, dr).wait_recv()
+                if (n, half) == (0, 0):
+                    out_wait(a, 0).wait_recv()
+                    out_wait(a, 1).wait_recv()
+                else:
+                    plane_wait(a, half, n, send, recv, ds, dr).wait_recv()
             picked.append(dot(pick_s[a], recv[a][n].reshape(512, WIDTHS[a])).astype(BF))
         acts = []
         for j in (0, 1):
@@ -427,43 +490,96 @@
                 ret[a][n, half] = done
                 if n == 0:
                     back[a][0, half, 0] = done[0]
-            plane_copies(half, n, ret, back, es, er, -1)
+            if (n, half) == (1, 0):
+                split_copies(1, 0, ret, back, es, er, -1)
+            else:
+                plane_copies(half, n, ret, back, es, er, -1)
 
     for one in b_copies.values():
         one.wait_send()
     p_copies = []
-    for half in (1, 0):
+
+    def plane_sum(a, half, cols):
+        return sum(
+            dot(
+                cw_s[2 * a + half, :, 256 * n : 256 * n + 256],
+                back[a][n, half, :, :, cols].reshape(256, cols.stop - cols.start),
+            )
+            for n in (0, 1)
+        )
+
+    for a in AXES:
+        for n in (0, 1):
+            plane_wait(a, 1, n, ret, back, es, er).wait_recv()
+        sum_a = plane_sum(a, 1, slice(0, WIDTHS[a]))
+        lines[a][2] = sum_a[0:128].astype(BF)
+        third_s[:, STARTS[a] : STARTS[a] + WIDTHS[a]] = sum_a[128:256]
+        for part, toward in ((0, 3), (1, 1)):
+            one = relay(
+                a, part, lines[a].at[2], sums[a].at[1], ps.at[8 * a + part], pr.at[8 * a + part],
+                toward,
+            )
+            one.start()
+            p_copies.append(one)
+    relayed = list(p_copies)
+    split_copies(1, 1, ret, back, es, er, -1)
+    for part in (0, 1):
         for a in AXES:
-            total_a = jnp.zeros((256, WIDTHS[a]), F32)
-            for n in (0, 1):
-                plane_wait(a, half, n, ret, back, es, er).wait_recv()
-                total_a = total_a + dot(
-                    cw_s[2 * a + half, :, 256 * n : 256 * n + 256],
-                    back[a][n, half].reshape(256, WIDTHS[a]),
+            cols = columns(a, part)
+            whole = slice(STARTS[a] + cols.start, STARTS[a] + cols.stop)
+            if part == 0:
+                plane_wait(a, 0, 0, ret, back, es, er).wait_recv()
+            last_wait(a, part).wait_recv()
+            sum_a = plane_sum(a, 0, cols)
+            shared_s[:, whole] += sum_a[0:128]
+            value = sum_a[128:256]
+            if part == 0:
+                relayed[2 * a].wait_recv()
+                value = value + sums[a][1, :, cols].astype(F32)
+            lines[a][1, :, cols] = value.astype(BF)
+            one = relay(
+                a, part, lines[a].at[1], sums[a].at[0], ps.at[8 * a + 2 + part],
+                pr.at[8 * a + 2 + part], 3,
+            )
+            one.start()
+            p_copies.append(one)
+        if part == 0:
+            for a in AXES:
+                cols = slice(FIRST[a], WIDTHS[a])
+                relayed[2 * a + 1].wait_recv()
+                value = third_s[:, STARTS[a] : STARTS[a] + WIDTHS[a]]
+                lines[a][3, :, 0 : FIRST[a]] = value[:, 0 : FIRST[a]].astype(BF)
+                lines[a][3, :, cols] = (value[:, cols] + sums[a][1, :, cols].astype(F32)).astype(BF)
+                one = pltpu.make_async_remote_copy(
+                    src_ref=lines[a].at[3], dst_ref=sums[a].at[2],
+                    send_sem=ps.at[8 * a + 4], recv_sem=pr.at[8 * a + 4],
+                    device_id=along(a, 1), device_id_type=MESH,
                 )
-            for d in (2 * half, 2 * half + 1):
-                mine = total_a[128 * (d % 2) : 128 * (d % 2) + 128]
-                if d == 0:
-                    cols = slice(STARTS[a], STARTS[a] + WIDTHS[a])
-                    shared_s[:, cols] += mine
-                else:
-                    lines[a][d] = mine.astype(BF)
-                    one = line_copy(a, d, lines[a].at[d], sums[a].at[d - 1], ps, pr, -1)
-                    one.start()
-                    p_copies.append(one)
+                one.start()
+                p_copies.append(one)
     for one in p_copies:
-        one.wait()
+        if not any(one is r for r in relayed):
+            one.wait_recv()
     for a in AXES:
         cols = slice(STARTS[a], STARTS[a] + WIDTHS[a])
         value = mid_s[:, cols].astype(F32) + shared_s[:, cols]
-        for d in range(3):
-            value = value + sums[a][d].astype(F32)
+        value = value + sums[a][0].astype(F32) + sums[a][2].astype(F32)
         out_ref[:, cols] = value.astype(BF)
+    for one in p_copies:
+        one.wait_send()
     for n in (0, 1):
         for half in (0, 1):
             for a in AXES:
-                plane_wait(a, half, n, send, recv, ds, dr).wait_send()
-                plane_wait(a, half, n, ret, back, es, er).wait_send()
+                if (n, half) == (0, 0):
+                    out_wait(a, 0).wait_send()
+                    out_wait(a, 1).wait_send()
+                else:
+                    plane_wait(a, half, n, send, recv, ds, dr).wait_send()
+                if (n, half) == (1, 0):
+                    last_wait(a, 0).wait_send()
+                    last_wait(a, 1).wait_send()
+                else:
+                    plane_wait(a, half, n, ret, back, es, er).wait_send()
 
 
 def on_device(
@@ -491,13 +607,14 @@
             V((2048, 512), BF), V((2048, 512), BF), V((512, 2048), BF),
             V((144, 128), BF), V((144, 128), BF), V((NY, 144, 128), BF), V((NZ, 144, 128), BF),
             V((2, 512, 128), F32), V((512, 128), BF), V((4, 128, 256), BF), V((4, 128, 256), BF),
-            V((128, 2048), BF), V((128, 2048), F32),
+            V((128, 2048), BF), V((128, 2048), F32), V((128, 2048), F32),
             V((12, 8, 128), F32), V((6, 512, 256), BF), V((6, 256, 512), BF),
             V((3, 512, 512), BF), V((3, 512, 512), BF),
             *[V((4, 128, w), BF) for w in WIDTHS], *[V((3, 128, w), BF) for w in WIDTHS],
             *[V((2, 2, 16, 16, w), BF) for _ in range(4) for w in WIDTHS],
             dma((13,)), dma, dma, dma((4,)), dma((4,)), dma((4,)), dma((4,)), dma((4,)), dma((4,)),
-            *[dma((12,)) for _ in range(10)],
+            dma((12,)), dma((12,)), dma((24,)), dma((24,)), *[dma((15,)) for _ in range(4)],
+            dma((24,)), dma((24,)),
         ],
         compiler_params=pltpu.CompilerParams(
             collective_id=0, has_side_effects=True, vmem_limit_bytes=62 * 1024 * 1024

time: 107 us -> 105 us (0.981)
  Pallas kernels: 105 us -> 102 us
    pallas_call x1, Pallas kernels: 105 us -> 102 us  [on_device(): pl.pallas_call(kernel, out_shape=jax.ShapeDtypeStruct((128, 2048), BF), i...]
where the time goes in v4:
time: 105 us; the launch traced here: 104 us
  Pallas kernels  102 us (97%)
  local copies, waits for them, and re-layouts  1.88 us (2%)
    pallas_call x1, Pallas kernels, on_device(): pl.pallas_call(kernel, out_shape=jax.ShapeDtypeStruct((128, 2048), BF), i...  102 us

profile of v4, /device:TPU:1, one launch (start us, length us, event | category | flops | bytes accessed | tf_op | source)
XLA Modules:
  0.0 103.9 jit_solution(3392528557613149557)
XLA Ops:
  0.0 102.0 %layer.1 = bf16[128,2048]{1,0:T(8,128)(2,1)} custom-call(bf16[512,128]{1,0:T(8,128)(2,1)} %q_hbm.1, bf16[512,128]{1,0:T(8,128)(2,1)} %k_hbm.1, bf16[512,256]{1,0:T(8,128)(2,1)} %v_hbm.1, bf16[512,128]{1,0:T(8,128)(2,1)} %cd_hbm.1, f32[2,512]{1,0:T(2,128)} %bitcast.6, bf16[512,256]{1,0:T(8,128)(2,1)} %og_hbm.1, f32[1,128]{1,0:T(1,128)} %bitcast.9, ...), custom_call_target="tpu_custom_call" | custom-call | tf_op jit(solution)/shard_map/layer/pallas_call | solution.py:595
  102.0 1.9 %copy.20 = bf16[128,2048]{1,0:T(8,128)(2,1)} copy(bf16[128,2048]{1,0:T(8,128)(2,1)} %layer.1) | data formatting | bytes 1048576

commit v5 on v4

--- a/solution.py
+++ b/solution.py
@@ -13,7 +13,7 @@
 BLOCK = 64
 NZ, NY, NC, NX = 4, 4, 2, 4
 DEVS = NZ * NY * NC * NX
-STEP = 5
+STEP = 11
 WIDTHS = (640, 640, 768)
 STARTS = (0, 640, 1280)
 FIRST = (384, 384, 384)

time: 105 us -> 105 us (level)
  no operation moved by 1% of the time
where the time goes in v5:
time: 105 us; the launch traced here: 104 us
  Pallas kernels  102 us (97%)
  local copies, waits for them, and re-layouts  1.88 us (2%)
    pallas_call x1, Pallas kernels, on_device(): pl.pallas_call(kernel, out_shape=jax.ShapeDtypeStruct((128, 2048), BF), i...  102 us

profile of v5, /device:TPU:1, one launch (start us, length us, event | category | flops | bytes accessed | tf_op | source)
XLA Modules:
  0.0 104.1 jit_solution(8262263162613499485)
XLA Ops:
  0.0 102.2 %layer.1 = bf16[128,2048]{1,0:T(8,128)(2,1)} custom-call(bf16[512,128]{1,0:T(8,128)(2,1)} %q_hbm.1, bf16[512,128]{1,0:T(8,128)(2,1)} %k_hbm.1, bf16[512,256]{1,0:T(8,128)(2,1)} %v_hbm.1, bf16[512,128]{1,0:T(8,128)(2,1)} %cd_hbm.1, f32[2,512]{1,0:T(2,128)} %bitcast.6, bf16[512,256]{1,0:T(8,128)(2,1)} %og_hbm.1, f32[1,128]{1,0:T(1,128)} %bitcast.9, ...), custom_call_target="tpu_custom_call" | custom-call | tf_op jit(solution)/shard_map/layer/pallas_call | solution.py:595
  102.2 1.9 %copy.20 = bf16[128,2048]{1,0:T(8,128)(2,1)} copy(bf16[128,2048]{1,0:T(8,128)(2,1)} %layer.1) | data formatting | bytes 1048576
